TPU v7x, 128 devices: a whole 4x4x4 slice. The times are simulated.
128 devices in a mesh: fs: 16 (over z, y), tp: 8 (over x, core).
Axes of the slice: x: 4, y: 4, z: 4, core: 2. Of those that a mesh axis runs over, the one named last changes fastest.
Arguments:
- saved_input: bfloat16 [262144, 2048], P(('fs', 'tp')), may hold values from -500 to 500
- value_cotangent: bfloat16 [262144, 1024], P(('fs', 'tp')), may hold values from -500 to 500
- hidden_input: bfloat16 [262144, 1024], P(('fs', 'tp')), may hold values from -500 to 500
- out_cotangent: bfloat16 [262144, 2048], P(('fs', 'tp')), may hold values from -500 to 500
- value_factor: bfloat16 [2048, 256], P('fs'), may hold values from -2 to 2
- out_factor: bfloat16 [1024, 256], P('fs'), may hold values from -2 to 2
- value_weight: float32 [2048, 1024], P('fs', 'tp'), may hold values from -0.125 to 0.125
- out_weight: float32 [1024, 2048], P('fs', 'tp'), may hold values from -0.1875 to 0.1875
- value_first: float32 [256, 1024], P('fs', 'tp'), may hold values from -1.2 to 1.2
- value_second: float32 [256, 1024], P('fs', 'tp'), may hold values from 0.02 to 0.5
- out_first: float32 [256, 2048], P('fs', 'tp'), may hold values from -1.2 to 1.2
- out_second: float32 [256, 2048], P('fs', 'tp'), may hold values from 0.02 to 0.5
Outputs:
- value_update: float32 [2048, 1024], P('fs', 'tp')
- out_update: float32 [1024, 2048], P('fs', 'tp')
- new_value_weight: float32 [2048, 1024], P('fs', 'tp')
- new_out_weight: float32 [1024, 2048], P('fs', 'tp')
- value_copy: bfloat16 [2048, 1024], P(None, 'tp')
- out_copy: bfloat16 [1024, 2048], P(None, 'tp')
- new_value_first: float32 [256, 1024], P('fs', 'tp')
- new_value_second: float32 [256, 1024], P('fs', 'tp')
- new_out_first: float32 [256, 2048], P('fs', 'tp')
- new_out_second: float32 [256, 2048], P('fs', 'tp')
All inputs are finite; a program needn't handle non-finite values.
Results may differ from a plain program's by a relative error of at most 0.0065.
Values may be sent and summed in bfloat16 or wider, within the bound.
No kernel may reach another device: no remote copies, remote signals or barrier semaphores. Data moves between devices by JAX's collectives and lax.ppermute only.
A program may use at most 128 MiB of HBM per device.

v0:
```python
import jax
import jax.numpy as jnp
from jax import lax
from jax.sharding import Mesh
from jax.sharding import PartitionSpec as P

D = 2048
DM = 1024
R = 256
FS = ("fs_0", "fs_1")
TP = ("tp_0", "tp_1")
FS_TP = ("fs_0", "fs_1", "tp_0", "tp_1")


momentum_decay = 0.9
square_decay = 0.95
adam_epsilon = 1e-08
update_scale = 0.25
learning_rate = 0.01


def copy_for_each(shard, axis):
    copies = jnp.broadcast_to(shard, (lax.axis_size(axis), *shard.shape))
    return lax.all_to_all(copies, axis, split_axis=0, concat_axis=0, tiled=True)


def laid_out(tiles, dim):
    tiles = jnp.moveaxis(tiles, 0, dim)
    lengths = tiles.shape
    return tiles.reshape(*lengths[:dim], lengths[dim] * lengths[dim + 1], *lengths[dim + 2 :])


def collect(shard, axis, dim):
    tiles = copy_for_each(shard, axis)
    return laid_out(tiles, dim)


def split_up(shard, dim, length):
    before, after = (shard.shape[:dim], shard.shape[dim + 1 :])
    return jnp.moveaxis(shard.reshape(*before, length, -1, *after), dim, 0)


def sum_at_owner(shard, axis, dim):
    length = lax.axis_size(axis)
    tiles = lax.all_to_all(split_up(shard, dim, length), axis, 0, 0, tiled=True)
    return jnp.sum(tiles.astype(jnp.float32), axis=0)


def sum_at_owner_2(shard, axis, dim):
    tiles = split_up(shard, dim, lax.axis_size(axis))
    arrived = lax.all_to_all(tiles, axis, split_axis=0, concat_axis=0, tiled=True)
    return arrived.sum(axis=0)


def over_axes(shard, axes):
    for axis in axes:
        shard = lax.psum(shard, axis)
    return shard


def side_by_side(arrays, axis, dim, along):
    ends, at = ([], 0)
    for a in arrays[:-1]:
        at += a.shape[along]
        ends.append(at)
    both = jnp.concatenate(arrays, axis=along)
    return tuple(jnp.split(lax.all_gather(both, axis, axis=dim, tiled=True), ends, axis=along))


def gather_packed(arrays, axis, dims):
    flat = jnp.concatenate([a.reshape(-1) for a in arrays])
    lines, at, outs = (lax.all_gather(flat, axis), 0, [])
    for a, dim in zip(arrays, dims):
        tiles = lines[:, at : at + a.size].reshape(-1, *a.shape)
        outs.append(laid_out(tiles, dim))
        at += a.size
    return tuple(outs)


def moment_ratio(first, second, lowrank, clip_factor):
    scaled = clip_factor * lowrank
    new_first = momentum_decay * first + (1.0 - momentum_decay) * scaled
    new_second = square_decay * second + (1.0 - square_decay) * scaled * scaled
    ratio = new_first / (jnp.sqrt(new_second) + adam_epsilon)
    return (new_first, new_second, ratio)


def input_times_factor(inputs, factor):
    return jnp.dot(inputs, collect(factor, FS, 0), preferred_element_type=jnp.float32)


def split_product(basis, cotangents):
    basis_high = basis.astype(jnp.bfloat16)
    basis_rest = (basis - basis_high.astype(jnp.float32)).astype(jnp.bfloat16)
    high_part = jnp.einsum("tr,tc->rc", basis_high, cotangents, preferred_element_type=jnp.float32)
    rest_part = jnp.einsum("tr,tc->rc", basis_rest, cotangents, preferred_element_type=jnp.float32)
    return high_part + rest_part


def shards(
    saved_input,
    value_cotangent,
    hidden_input,
    out_cotangent,
    value_factor,
    out_factor,
    value_weight,
    out_weight,
    value_first,
    value_second,
    out_first,
    out_second,
):
    highest = lax.Precision.HIGHEST
    value_basis = input_times_factor(saved_input, value_factor)
    out_basis = input_times_factor(hidden_input, out_factor)
    left = value_basis
    right = out_basis
    first_part = split_product(left, value_cotangent)
    second_part = split_product(right, out_cotangent)
    lowrank = sum_at_owner(
        jnp.concatenate([first_part, second_part], axis=1).astype(jnp.bfloat16), FS, 0
    )
    low_value, low_out = (
        sum_at_owner_2(lowrank[:, :DM], TP, 1),
        sum_at_owner_2(lowrank[:, DM:], TP, 1),
    )
    squares = (
        over_axes(jnp.sum(low_value * low_value), FS_TP),
        over_axes(jnp.sum(low_out * low_out), FS_TP),
    )
    root_mean = jnp.sqrt((squares[0] + squares[1]) / (R * (D + DM)))
    clip_factor = 1.0 / jnp.maximum(root_mean, 1.0)
    new_value_first, new_value_second, value_ratio = moment_ratio(
        value_first, value_second, low_value, clip_factor
    )
    new_out_first, new_out_second, out_ratio = moment_ratio(
        out_first, out_second, low_out, clip_factor
    )
    pieces = side_by_side((value_ratio, out_ratio), FS, 0, 1)
    left = value_factor.astype(jnp.float32)
    right = out_factor.astype(jnp.float32)
    value_sum = jnp.dot(left, pieces[0], precision=highest)
    out_sum = jnp.dot(right, pieces[1], precision=highest)
    value_update = update_scale * value_sum
    out_update = update_scale * out_sum
    new_value_weight = value_weight - learning_rate * value_update
    new_out_weight = out_weight - learning_rate * out_update
    value_copy, out_copy = gather_packed(
        (new_value_weight.astype(jnp.bfloat16), new_out_weight.astype(jnp.bfloat16)), FS, (0, 0)
    )
    return (
        value_update,
        out_update,
        new_value_weight,
        new_out_weight,
        value_copy,
        out_copy,
        new_value_first,
        new_value_second,
        new_out_first,
        new_out_second,
    )


def solution(mesh):
    torus = Mesh(mesh.devices.reshape(4, 4, 4, 2), ("fs_0", "fs_1", "tp_0", "tp_1"))
    return jax.shard_map(
        shards,
        mesh=torus,
        in_specs=(
            P(FS_TP, None),
            P(FS_TP, None),
            P(FS_TP, None),
            P(FS_TP, None),
            P(FS, None),
            P(FS, None),
            P(FS, TP),
            P(FS, TP),
            P(FS, TP),
            P(FS, TP),
            P(FS, TP),
            P(FS, TP),
        ),
        out_specs=(
            P(FS, TP),
            P(FS, TP),
            P(FS, TP),
            P(FS, TP),
            P(None, TP),
            P(None, TP),
            P(FS, TP),
            P(FS, TP),
            P(FS, TP),
            P(FS, TP),
        ),
        check_vma=False,
    )
```

profile of v0, /device:TPU:0, one launch (start us, length us, event | category | flops | bytes accessed | tf_op | source)
XLA Modules:
  0.0 212.2 jit_solution(17302194149277601238)
XLA Ops:
  7.2 0.8 broadcast_in_dim.7
  8.0 19.5 %all_to_all.25 = bf16[16,64,256]{2,1,0:T(8,128)(2,1)S(1)} all-to-all(bf16[16,64,256]{2,1,0:T(8,128)(2,1)S(1)} %broadcast_in_dim.7), channel_id=1, replica_groups=mesh['fs_0'=4,'fs_1'=4,'tp_0'=4,'tp_1'=2] {'fs_0','fs_1'}, dimensions={0} | all-to-all | bytes 1048576 | tf_op jit(solution)/shard_map/all_to_all | solution.py:24
  27.5 1.9 broadcast_in_dim.6
  29.4 3.7 %all-to-all-start = ((bf16[16,128,256]{2,1,0:T(8,128)(2,1)}), bf16[16,128,256]{2,1,0:T(8,128)(2,1)S(1)}, u32[]{:S(2)}, u32[]{:S(2)}) async-start(bf16[16,128,256]{2,1,0:T(8,128)(2,1)} %broadcast_in_dim.6), calls=%async_computation | async-start | bytes 2097152 | tf_op jit(solution)/shard_map/all_to_all | solution.py:24
  33.1 3.6 %fusion.19 = f32[2048,256]{1,0:T(8,128)S(1)} fusion(bf16[2048,1024]{1,0:T(8,128)(2,1)} %param.14, bf16[1024,256]{1,0:T(8,128)(2,1)S(1)} %bitcast.41), kind=kOutput, calls=%fused_computation.39 | convolution fusion | flops 1073741824 | bytes 6815744 | tf_op jit(solution)/shard_map/dot_general | solution.py:89
  36.7 5.9 %fusion.3 = f32[256,2048]{1,0:T(8,128)S(1)} fusion(bf16[2048,2048]{1,0:T(8,128)(2,1)} %param.15, f32[2048,256]{1,0:T(8,128)S(1)} %fusion.19), kind=kOutput, calls=%fused_computation.9 | convolution fusion | flops 2148007936 | bytes 12582912 | tf_op jit(solution)/shard_map/tr,tc->rc/dot_general | solution.py:95
  42.6 2.4 %fusion = bf16[256,2048]{1,0:T(8,128)(2,1)S(1)} fusion(f32[256,2048]{1,0:T(8,128)S(1)} %fusion.3, bf16[2048,2048]{1,0:T(8,128)(2,1)S(1)} %bitcast.38, f32[2048,256]{1,0:T(8,128)S(1)} %fusion.19), kind=kOutput, calls=%fused_computation.2 | convolution fusion | flops 2150629376 | bytes 13631488 | tf_op jit(solution)/shard_map/tr,tc->rc/dot_general | solution.py:96
  45.0 4.4 %all-to-all-done = bf16[16,128,256]{2,1,0:T(8,128)(2,1)S(1)} async-done(((bf16[16,128,256]{2,1,0:T(8,128)(2,1)}), bf16[16,128,256]{2,1,0:T(8,128)(2,1)S(1)}, u32[]{:S(2)}, u32[]{:S(2)}) %all-to-all-start) | async-done | bytes 1048608 | tf_op jit(solution)/shard_map/all_to_all | solution.py:24
  49.4 6.0 %fusion.18 = f32[2048,256]{1,0:T(8,128)S(1)} fusion(bf16[2048,2048]{1,0:T(8,128)(2,1)} %param.12, bf16[2048,256]{1,0:T(8,128)(2,1)S(1)} %bitcast.40), kind=kOutput, calls=%fused_computation.38 | convolution fusion | flops 2147483648 | bytes 11534336 | tf_op jit(solution)/shard_map/dot_general | solution.py:89
  55.4 1.3 fusion.6
  56.7 1.3 fusion.1
  58.1 25.1 %all_to_all.26 = bf16[16,16,3072]{2,1,0:T(8,128)(2,1)S(1)} all-to-all(bf16[16,16,3072]{2,1,0:T(8,128)(2,1)S(1)} %pad_maximum_fusion), channel_id=1, replica_groups=mesh['fs_0'=4,'fs_1'=4,'tp_0'=4,'tp_1'=2] {'fs_0','fs_1'}, dimensions={0} | all-to-all | bytes 3145728 | tf_op jit(solution)/shard_map/all_to_all | solution.py:45
  83.5 0.6 copy.33
  84.2 4.3 %all-to-all-start.3 = ((f32[8,16,128]{2,1,0:T(8,128)}), f32[8,16,128]{2,1,0:T(8,128)S(1)}, u32[]{:S(2)}, u32[]{:S(2)}) async-start(f32[8,16,128]{2,1,0:T(8,128)} %copy.33), calls=%async_computation.3 | async-start | bytes 131072 | tf_op jit(solution)/shard_map/all_to_all | solution.py:51
  88.5 0.7 copy.34
  89.2 4.9 %all-to-all-done.3 = f32[8,16,128]{2,1,0:T(8,128)S(1)} async-done(((f32[8,16,128]{2,1,0:T(8,128)}), f32[8,16,128]{2,1,0:T(8,128)S(1)}, u32[]{:S(2)}, u32[]{:S(2)}) %all-to-all-start.3) | async-done | bytes 65568 | tf_op jit(solution)/shard_map/all_to_all | solution.py:51
  94.1 3.4 %all-to-all-start.4 = ((f32[8,16,256]{2,1,0:T(8,128)}), f32[8,16,256]{2,1,0:T(8,128)S(1)}, u32[]{:S(2)}, u32[]{:S(2)}) async-start(f32[8,16,256]{2,1,0:T(8,128)} %copy.34), calls=%async_computation.4 | async-start | bytes 262144 | tf_op jit(solution)/shard_map/all_to_all | solution.py:51
  98.1 5.4 %all-to-all-done.4 = f32[8,16,256]{2,1,0:T(8,128)S(1)} async-done(((f32[8,16,256]{2,1,0:T(8,128)}), f32[8,16,256]{2,1,0:T(8,128)S(1)}, u32[]{:S(2)}, u32[]{:S(2)}) %all-to-all-start.4) | async-done | bytes 131104 | tf_op jit(solution)/shard_map/all_to_all | solution.py:51
  105.4 9.1 %psum.67 = f32[]{:T(128)} all-reduce(f32[]{:T(128)S(6)} %add.51), channel_id=1, replica_groups=mesh['fs_0'=4,'fs_1'=4,'tp_0'=4,'tp_1'=2] {'fs_0'}, use_global_device_ids=true, to_apply=%region_3.0 | all-reduce | flops 1 | bytes 8 | tf_op jit(solution)/shard_map/psum | solution.py:57
  114.5 9.2 %psum.66 = f32[]{:T(128)} all-reduce(f32[]{:T(128)} %psum.67), channel_id=1, replica_groups=mesh['fs_0'=4,'fs_1'=4,'tp_0'=4,'tp_1'=2] {'fs_1'}, use_global_device_ids=true, to_apply=%region_4.0 | all-reduce | flops 1 | bytes 8 | tf_op jit(solution)/shard_map/psum | solution.py:57
  123.7 9.5 %psum.65 = f32[]{:T(128)} all-reduce(f32[]{:T(128)} %psum.66), channel_id=1, replica_groups=mesh['fs_0'=4,'fs_1'=4,'tp_0'=4,'tp_1'=2] {'tp_0'}, use_global_device_ids=true, to_apply=%region_5.0 | all-reduce | flops 1 | bytes 8 | tf_op jit(solution)/shard_map/psum | solution.py:57
  133.3 3.1 %psum.64 = f32[]{:T(128)} all-reduce(f32[]{:T(128)} %psum.65), channel_id=1, replica_groups=mesh['fs_0'=4,'fs_1'=4,'tp_0'=4,'tp_1'=2] {'tp_1'}, use_global_device_ids=true, to_apply=%region_6.0 | all-reduce | flops 1 | bytes 8 | tf_op jit(solution)/shard_map/psum | solution.py:57
  138.4 22.0 %all_gather.9 = f32[256,384]{1,0:T(8,128)S(1)} all-gather(f32[16,384]{1,0:T(8,128)S(1)} %pad_maximum_fusion.2), channel_id=1, replica_groups=mesh['fs_0'=4,'fs_1'=4,'tp_0'=4,'tp_1'=2] {'fs_0','fs_1'}, dimensions={0}, use_global_device_ids=true | all-gather | bytes 417792 | tf_op jit(solution)/shard_map/all_gather | solution.py:67
  160.9 0.6 convert_bitcast_fusion
  161.7 0.6 pad_maximum_fusion.1
  162.4 0.7 copy.37
  163.1 0.7 copy.38
  163.8 0.6 multiply_bitcast_fusion
  164.5 37.2 %all-gather.3.cloned.1.call-done = bf16[524288]{0:T(1024)(128)(2,1)} async-done(((bf16[32768]{0:T(1024)(128)(2,1)}), bf16[524288]{0:T(1024)(128)(2,1)}) %all-gather.3.cloned.1.call-update) | async-done | bytes 1048592 | tf_op jit(solution)/shard_map/all_gather | solution.py:72
  201.7 1.5 reshape.49
  203.3 1.0 reshape_reshape.6
  204.4 1.0 reshape_reshape.7
  (45 shorter events, 3.8 us)
Async XLA Ops:
  29.4 19.9 %all-to-all-start = ((bf16[16,128,256]{2,1,0:T(8,128)(2,1)}), bf16[16,128,256]{2,1,0:T(8,128)(2,1)S(1)}, u32[]{:S(2)}, u32[]{:S(2)}) async-start(bf16[16,128,256]{2,1,0:T(8,128)(2,1)} %broadcast_in_dim.6), calls=%async_computation | async-start | bytes 2097152 | tf_op jit(solution)/shard_map/all_to_all | solution.py:24
  33.1 9.5 %slice-start = ((s8[8388608]{0:T(1024)(128)(4,1)}), s8[4194304]{0:T(1024)(128)(4,1)S(1)}, s32[]{:S(2)}) async-start(s8[8388608]{0:T(1024)(128)(4,1)} %bitcast.37), calls=%async_computation.6 | async-start | bytes 8388608
  36.7 5.9 %slice-start.1 = ((s8[8388608]{0:T(1024)(128)(4,1)}), s8[4194304]{0:T(1024)(128)(4,1)S(1)}, s32[]{:S(2)}) async-start(s8[8388608]{0:T(1024)(128)(4,1)} %bitcast.37), calls=%async_computation.7 | async-start | bytes 8388608
  49.4 6.0 %copy-start.8 = (bf16[2048,1024]{1,0:T(8,128)(2,1)S(1)}, bf16[2048,1024]{1,0:T(8,128)(2,1)}, u32[]{:S(2)}) copy-start(bf16[2048,1024]{1,0:T(8,128)(2,1)} %param.13) | copy-start | bytes 12582916
  83.2 50.0 %copy-start.3 = (f32[128,128]{1,0:T(8,128)S(1)}, f32[128,128]{1,0:T(8,128)}, u32[]{:S(2)}) copy-start(f32[128,128]{1,0:T(8,128)} %param.18) | copy-start | bytes 196612
  83.2 53.9 %copy-start.4 = (f32[16,256]{1,0:T(8,128)S(1)}, f32[16,256]{1,0:T(8,128)}, u32[]{:S(2)}) copy-start(f32[16,256]{1,0:T(8,128)} %param.23) | copy-start | bytes 49156
  83.2 54.0 %copy-start.5 = (f32[16,256]{1,0:T(8,128)S(1)}, f32[16,256]{1,0:T(8,128)}, u32[]{:S(2)}) copy-start(f32[16,256]{1,0:T(8,128)} %param.22) | copy-start | bytes 49156
  83.2 54.6 %copy-start.6 = (f32[16,128]{1,0:T(8,128)S(1)}, f32[16,128]{1,0:T(8,128)}, u32[]{:S(2)}) copy-start(f32[16,128]{1,0:T(8,128)} %param.21) | copy-start | bytes 24580
  83.2 54.6 %copy-start.7 = (f32[16,128]{1,0:T(8,128)S(1)}, f32[16,128]{1,0:T(8,128)}, u32[]{:S(2)}) copy-start(f32[16,128]{1,0:T(8,128)} %param.20) | copy-start | bytes 24580
  83.2 77.1 %copy-start.1 = (bf16[64,256]{1,0:T(8,128)(2,1)S(1)}, bf16[64,256]{1,0:T(8,128)(2,1)}, u32[]{:S(2)}) copy-start(bf16[64,256]{1,0:T(8,128)(2,1)} %param.17) | copy-start | bytes 98308
  83.2 77.4 %copy-start = (bf16[128,256]{1,0:T(8,128)(2,1)S(1)}, bf16[128,256]{1,0:T(8,128)(2,1)}, u32[]{:S(2)}) copy-start(bf16[128,256]{1,0:T(8,128)(2,1)} %param.16) | copy-start | bytes 196612
  83.5 77.4 %copy-start.2 = (f32[64,256]{1,0:T(8,128)S(1)}, f32[64,256]{1,0:T(8,128)}, u32[]{:S(2)}) copy-start(f32[64,256]{1,0:T(8,128)} %param.19) | copy-start | bytes 196612
  84.2 9.9 %all-to-all-start.3 = ((f32[8,16,128]{2,1,0:T(8,128)}), f32[8,16,128]{2,1,0:T(8,128)S(1)}, u32[]{:S(2)}, u32[]{:S(2)}) async-start(f32[8,16,128]{2,1,0:T(8,128)} %copy.33), calls=%async_computation.3 | async-start | bytes 131072 | tf_op jit(solution)/shard_map/all_to_all | solution.py:51
  94.1 9.4 %all-to-all-start.4 = ((f32[8,16,256]{2,1,0:T(8,128)}), f32[8,16,256]{2,1,0:T(8,128)S(1)}, u32[]{:S(2)}, u32[]{:S(2)}) async-start(f32[8,16,256]{2,1,0:T(8,128)} %copy.34), calls=%async_computation.4 | async-start | bytes 262144 | tf_op jit(solution)/shard_map/all_to_all | solution.py:51
  97.5 104.3 %all-gather.3.cloned.1.call-start = ((), (), s32[]{:S(2)}) async-start(), calls=%async_computation.5 | async-start | bytes 1114112 | tf_op jit(solution)/shard_map/all_gather | solution.py:72
Sparse Core Ops, SparseCore 0:
  162.5 39.1 all-gather.2
where the time goes:
time: 213 us; the launch traced here: 212 us
  blocking collectives  97.5 us (46%)
  waiting for transfers between devices  51.9 us (24%)
  matrix products  20.9 us (10%)
  between operations  16.4 us (8%)
  starting transfers between devices  11.4 us (5%)
  local copies, waits for them, and re-layouts  9.54 us (4%)
  other arithmetic  4.73 us (2%)
    all_gather x1, waiting for transfers between devices, gather_packed(): lines, at, outs = (lax.all_gather(flat, axis), 0, [])  37.2 us
    psum x4, blocking collectives, over_axes(): shard = lax.psum(shard, axis)  30.9 us
    all_to_all x1, blocking collectives, sum_at_owner(): tiles = lax.all_to_all(split_up(shard, dim, length), axis, 0, 0, tiled=True)  25.1 us
    all_gather x1, blocking collectives, side_by_side(): lax.all_gather(both, axis, axis=dim, tiled=True)  22 us
    all_to_all x1, blocking collectives, copy_for_each(): return lax.all_to_all(copies, axis, split_axis=0, concat_axis=0, tiled=True)  19.5 us
    all_to_all x2, waiting for transfers between devices, sum_at_owner_2(): lax.all_to_all(tiles, axis, split_axis=0, concat_axis=0, tiled=True)  10.2 us
    dot_general x2, matrix products, input_times_factor(): jnp.dot(inputs, collect(factor, FS, 0), preferred_element_type=jnp.float32)  9.6 us
    all_to_all x2, starting transfers between devices, sum_at_owner_2(): lax.all_to_all(tiles, axis, split_axis=0, concat_axis=0, tiled=True)  7.67 us
  transfers between devices with their start and end apart: 4, of which 4 were waited for; matrix products, arithmetic and copies ran while one was open for 7% of the time, Pallas kernels for 0%

commit v1 on v0

v1 whole, which is shorter than its diff:
```python
import jax
import jax.numpy as jnp
from jax import lax
from jax.sharding import Mesh
from jax.sharding import PartitionSpec as P

D = 2048
DM = 1024
R = 256
FS = ("fs_0", "fs_1")
TP = ("tp_0", "tp_1")
CHIPS = ("fs_0", "fs_1", "tp_0")
CORE = "tp_1"
FS_TP = ("fs_0", "fs_1", "tp_0", "tp_1")
HALF = R // 2

momentum_decay = 0.9
square_decay = 0.95
adam_epsilon = 1e-08
update_scale = 0.25
learning_rate = 0.01

bf16 = jnp.bfloat16
f32 = jnp.float32


def exchange(tiles, axis):
    return lax.all_to_all(tiles, axis, split_axis=0, concat_axis=0, tiled=True)


def to_each(block, axis):
    return exchange(jnp.broadcast_to(block, (lax.axis_size(axis), *block.shape)), axis)


def partner(x):
    return lax.ppermute(x, CORE, [(0, 1), (1, 0)])


def side(a):
    return jnp.concatenate([a[:, :128], a[:, 128:]], axis=0)


def unside(a, rows):
    a = a.reshape(16, 2, rows, 128)
    return a.transpose(0, 2, 1, 3).reshape(16 * rows, 256)


def split_dot(factor, ratio):
    high = ratio.astype(bf16)
    rest = (ratio - high.astype(f32)).astype(bf16)
    return jnp.dot(factor, high, preferred_element_type=f32) + jnp.dot(
        factor, rest, preferred_element_type=f32
    )


def moments(first, second, scaled):
    new_first = momentum_decay * first + (1.0 - momentum_decay) * scaled
    new_second = square_decay * second + (1.0 - square_decay) * scaled * scaled
    return new_first, new_second


def columns(a, core):
    width = a.shape[1] // 8
    a = a.reshape(32, 4, 4, 2, width)
    a = jnp.where(core == 0, a, a[:, :, :, ::-1])
    return a.transpose(0, 3, 2, 1, 4)


def shards(
    saved_input,
    value_cotangent,
    hidden_input,
    out_cotangent,
    value_factor,
    out_factor,
    value_weight,
    out_weight,
    value_first,
    value_second,
    out_first,
    out_second,
):
    core = lax.axis_index(CORE)
    row = lax.axis_index(FS)
    factors = jnp.concatenate([value_factor, out_factor], axis=0)
    mine = lax.dynamic_slice(factors, (0, HALF * core), (192, HALF))
    block = jnp.concatenate(
        [
            mine,
            value_weight.astype(bf16),
            side(out_weight.astype(bf16)),
            value_first.astype(bf16),
            value_second.astype(bf16),
            side(out_first.astype(bf16)),
            side(out_second.astype(bf16)),
        ],
        axis=0,
    )
    got = to_each(block, FS)
    factor_mine = got[:, :192]
    factor_other = partner(factor_mine)
    factor = jnp.concatenate([factor_mine, factor_other], axis=2)
    value_f = factor[:, :128].reshape(D, R)
    out_f = factor[:, 128:].reshape(DM, R)
    value_w = got[:, 192:320].reshape(D, 128)
    out_w = unside(got[:, 320:448], 64)
    first_v = got[:, 448:464].reshape(R, 128)
    second_v = got[:, 464:480].reshape(R, 128)
    first_o = unside(got[:, 480:512], 16)
    second_o = unside(got[:, 512:544], 16)

    value_basis = jnp.dot(saved_input, value_f, preferred_element_type=f32).astype(bf16)
    out_basis = jnp.dot(hidden_input, out_f, preferred_element_type=f32).astype(bf16)
    part_v = jnp.einsum("tr,tc->rc", value_basis, value_cotangent, preferred_element_type=f32)
    part_o = jnp.einsum("tr,tc->rc", out_basis, out_cotangent, preferred_element_type=f32)
    sent = jnp.concatenate([part_v[HALF:], part_o[HALF:]], axis=1).astype(bf16)
    came = partner(sent).astype(f32)
    sum_v = (part_v[:HALF] + came[:, :DM]).astype(bf16)
    sum_o = (part_o[:HALF] + came[:, DM:]).astype(bf16)
    tiles = jnp.concatenate([columns(sum_v, core), columns(sum_o, core)], axis=4)
    owned = jnp.sum(exchange(tiles.reshape(64, 16, 384), CHIPS).astype(f32), axis=0)

    squares = jnp.broadcast_to(jnp.sum(owned * owned), (4, 4, 128))
    reply = jnp.concatenate([owned.reshape(4, 12, 128), squares], axis=1)
    replies = jnp.broadcast_to(reply, (16, 4, 16, 128)).reshape(64, 16, 128)
    back = exchange(replies, CHIPS)
    low_mine = back[:, :12].reshape(32, 2, 4, 384)
    ss_mine = jnp.sum(back[:, 12, 0])
    low_kept = low_mine[:, 0].reshape(HALF, 384)
    gone = jnp.concatenate(
        [low_mine[:, 1].reshape(HALF, 384), jnp.broadcast_to(ss_mine, (8, 384))], axis=0
    )
    gone = partner(gone)
    low_other = gone[:HALF]
    total = ss_mine + gone[HALF, 0]
    root_mean = jnp.sqrt(total / (R * (D + DM)))
    clip_factor = 1.0 / jnp.maximum(root_mean, 1.0)
    return low_kept, low_other, clip_factor, value_f, out_f, value_w, out_w, first_v, second_v, first_o, second_o, core, row, (value_weight, out_weight, value_first, value_second, out_first, out_second)


def finish(low_kept, low_other, clip_factor, value_f, out_f, value_w, out_w, first_v, second_v, first_o, second_o, core, row, own):
    value_weight, out_weight, value_first, value_second, out_first, out_second = own
    low = jnp.where(
        core == 0,
        jnp.concatenate([low_kept, low_other], axis=0),
        jnp.concatenate([low_other, low_kept], axis=0),
    )
    scaled = clip_factor * low
    own_scaled = lax.dynamic_slice(scaled, (16 * row, 0), (16, 384))
    new_value_first, new_value_second = moments(value_first, value_second, own_scaled[:, :128])
    new_out_first, new_out_second = moments(out_first, out_second, own_scaled[:, 128:])
    m_v, s_v = moments(first_v.astype(f32), second_v.astype(f32), scaled[:, :128])
    m_o, s_o = moments(first_o.astype(f32), second_o.astype(f32), scaled[:, 128:])
    ratio_v = m_v / (jnp.sqrt(s_v) + adam_epsilon)
    ratio_o = m_o / (jnp.sqrt(s_o) + adam_epsilon)

    def mine_first(a):
        return jnp.where(core == 0, a, jnp.concatenate([a[HALF:], a[:HALF]], axis=0))

    value_all = update_scale * split_dot(value_f, mine_first(ratio_v))
    out_all = update_scale * split_dot(out_f, mine_first(ratio_o))
    value_copy = (value_w.astype(f32) - learning_rate * value_all).astype(bf16)
    out_copy = (out_w.astype(f32) - learning_rate * out_all).astype(bf16)
    value_update = lax.dynamic_slice(value_all, (128 * row, 0), (128, 128))
    out_update = lax.dynamic_slice(out_all, (64 * row, 0), (64, 256))
    return (
        value_update,
        out_update,
        value_weight - learning_rate * value_update,
        out_weight - learning_rate * out_update,
        value_copy,
        out_copy,
        new_value_first,
        new_value_second,
        new_out_first,
        new_out_second,
    )


def step(*args):
    return finish(*shards(*args))


def solution(mesh):
    torus = Mesh(mesh.devices.reshape(4, 4, 4, 2), FS_TP)
    return jax.shard_map(
        step,
        mesh=torus,
        in_specs=(P(FS_TP, None),) * 4 + (P(FS, None),) * 2 + (P(FS, TP),) * 6,
        out_specs=(P(FS, TP),) * 4 + (P(None, TP),) * 2 + (P(FS, TP),) * 4,
        check_vma=False,
    )
```

time: 213 us -> 159 us (0.75)
  waiting for transfers between devices: 51.9 us -> 13.7 us
  blocking collectives: 97.5 us -> 60.8 us
  local copies, waits for them, and re-layouts: 9.54 us -> 28 us
  other arithmetic: 4.73 us -> 23 us
  between operations: 16.4 us -> 2.32 us
  starting transfers between devices: 11.4 us -> 5.89 us
    all_gather x1 -> x0, waiting for transfers between devices: 37.2 us -> none  [gather_packed(): lines, at, outs = (lax.all_gather(flat, axis), 0, [])]
    psum x4 -> x0, blocking collectives: 30.9 us -> none  [over_axes(): shard = lax.psum(shard, axis)]
    all_gather x1 -> x0, blocking collectives: 22 us -> none  [side_by_side(): lax.all_gather(both, axis, axis=dim, tiled=True)]
    all_to_all x2, blocking collectives: 44.6 us -> 60.8 us  [exchange(): return lax.all_to_all(tiles, axis, split_axis=0, concat_axis=0, tiled=True)]
    reshape x0 -> x7, local copies, waits for them, and re-layouts: none -> 9.67 us  [the longest x4 5.42 us: columns(): a = a.reshape(32, 4, 4, 2, width)]
    slice x2 -> x9, local copies, waits for them, and re-layouts: 0.08 us -> 8.1 us  [the longest x2 3.15 us: shards(): sent = jnp.concatenate([part_v[HALF:], part_o[HALF:]], axis=1).astype(bf16)]
    all_to_all x3 -> x1, waiting for transfers between devices: 14.6 us -> 8.84 us  [exchange(): return lax.all_to_all(tiles, axis, split_axis=0, concat_axis=0, tiled=True)]
    all_to_all x3 -> x1, starting transfers between devices: 11.3 us -> 5.66 us  [exchange(): return lax.all_to_all(tiles, axis, split_axis=0, concat_axis=0, tiled=True)]
  transfers between devices with their start and end apart: 4 -> 4, of which waited for: 4 -> 4; matrix products, arithmetic and copies ran while one was open for 7% -> 3% of each run, Pallas kernels for 0% -> 0%
where the time goes in v1:
time: 159 us; the launch traced here: 156 us
  blocking collectives  60.8 us (38%)
  local copies, waits for them, and re-layouts  28 us (18%)
  other arithmetic  23 us (14%)
  matrix products  22.8 us (14%)
  waiting for transfers between devices  13.7 us (9%)
  starting transfers between devices  5.89 us (4%)
  between operations  2.32 us (1%)
    all_to_all x2, blocking collectives, exchange(): return lax.all_to_all(tiles, axis, split_axis=0, concat_axis=0, tiled=True)  60.8 us
    dot_general x1, matrix products, shards(): jnp.einsum('tr,tc->rc', out_basis, out_cotangent, preferred_element_type=...  9.62 us
    dot_general x1, matrix products, shards(): jnp.einsum('tr,tc->rc', value_basis, value_cotangent, preferred_element_t...  9.01 us
    all_to_all x1, waiting for transfers between devices, exchange(): return lax.all_to_all(tiles, axis, split_axis=0, concat_axis=0, tiled=True)  8.84 us
    all_to_all x1, starting transfers between devices, exchange(): return lax.all_to_all(tiles, axis, split_axis=0, concat_axis=0, tiled=True)  5.66 us
    reshape x4, local copies, waits for them, and re-layouts, columns(): a = a.reshape(32, 4, 4, 2, width)  5.42 us
    ppermute x3, waiting for transfers between devices, partner(): return lax.ppermute(x, CORE, [(0, 1), (1, 0)])  4.83 us
  transfers between devices with their start and end apart: 4, of which 4 were waited for; matrix products, arithmetic and copies ran while one was open for 3% of the time, Pallas kernels for 0%

profile of v1, /device:TPU:0, one launch (start us, length us, event | category | flops | bytes accessed | tf_op | source)
XLA Modules:
  0.0 156.5 jit_solution(8824078092595158802)
XLA Ops:
  6.3 37.8 %all_to_all.15 = bf16[16,544,128]{2,1,0:T(8,128)(2,1)S(1)} all-to-all(bf16[16,544,128]{2,1,0:T(8,128)(2,1)S(1)} %broadcast_in_dim.8), channel_id=1, replica_groups=mesh['fs_0'=4,'fs_1'=4,'tp_0'=4,'tp_1'=2] {'fs_0','fs_1'}, dimensions={0} | all-to-all | bytes 4456448 | tf_op jit(solution)/shard_map/all_to_all | solution.py:28
  44.2 2.3 %collective-permute-done = bf16[16,192,128]{2,1,0:T(8,128)(2,1)S(1)} collective-permute-done((bf16[16,192,128]{2,1,0:T(8,128)(2,1)S(1)}, bf16[16,192,128]{2,1,0:T(8,128)(2,1)S(1)}, u32[]{:S(2)}, u32[]{:S(2)}) %collective-permute-start) | collective-permute-done | bytes 786464 | tf_op jit(solution)/shard_map/ppermute | solution.py:36
  48.3 9.6 %fusion.4 = f32[256,2048]{1,0:T(8,128)} fusion(bf16[2048,2048]{1,0:T(8,128)(2,1)} %param.15, bf16[1024,256]{1,0:T(8,128)(2,1)} %bitcast.54, bf16[2048,1024]{1,0:T(8,128)(2,1)} %param.14), kind=kOutput, calls=%fused_computation.18 | convolution fusion | flops 3221749760 | bytes 15204352 | tf_op jit(solution)/shard_map/tr,tc->rc/dot_general | solution.py:115
  57.9 2.1 %slice.204 = bf16[128,2048]{1,0:T(8,128)(2,1)} slice(f32[256,2048]{1,0:T(8,128)} %fusion.4), slice={[128:256], [0:2048]} | slice | bytes 1048576 | tf_op jit(solution)/shard_map/slice | solution.py:116
  60.0 1.3 fusion
  61.3 9.0 %fusion.5 = f32[256,1024]{1,0:T(8,128)} fusion(bf16[2048,1024]{1,0:T(8,128)(2,1)} %param.13, bf16[2048,256]{1,0:T(8,128)(2,1)S(1)} %bitcast.51, bf16[2048,2048]{1,0:T(8,128)(2,1)} %param.12), kind=kOutput, calls=%fused_computation.19 | convolution fusion | flops 3221749760 | bytes 14680064 | tf_op jit(solution)/shard_map/tr,tc->rc/dot_general | solution.py:114
  70.3 1.1 slice.205
  71.4 2.0 %pad_maximum_fusion = bf16[128,3072]{1,0:T(8,128)(2,1)} fusion(bf16[128,2048]{1,0:T(8,128)(2,1)} %slice.204, bf16[128,1024]{1,0:T(8,128)(2,1)S(1)} %slice.205), kind=kLoop, calls=%fused_computation.15 | loop fusion | flops 1572864 | bytes 1572864 | tf_op jit(solution)/shard_map/concatenate | solution.py:116
  73.5 2.5 %collective-permute-done.1 = bf16[128,3072]{1,0:T(8,128)(2,1)} collective-permute-done((bf16[128,3072]{1,0:T(8,128)(2,1)}, bf16[128,3072]{1,0:T(8,128)(2,1)}, u32[]{:S(2)}, u32[]{:S(2)}) %collective-permute-start.1) | collective-permute-done | bytes 786464 | tf_op jit(solution)/shard_map/ppermute | solution.py:36
  76.0 1.3 convert_element_type.110
  77.3 1.1 fusion.7
  80.2 1.1 copy.26
  81.3 2.2 %reshape.80 = bf16[32,4,4,2,256]{4,3,2,1,0:T(2,128)(2,1)} reshape(bf16[128,2048]{1,0:T(8,128)(2,1)} %fusion.2) | data formatting | bytes 1048576 | tf_op jit(solution)/shard_map/reshape | solution.py:64
  83.5 1.3 copy.28
  85.2 1.3 pad_maximum_fusion.1
  86.5 2.3 %reshape.81 = bf16[64,16,384]{2,1,0:T(8,128)(2,1)} reshape(bf16[32,2,4,4,384]{4,3,2,1,0:T(4,128)(2,1)} %pad_maximum_fusion.1) | data formatting | bytes 1572864 | tf_op jit(solution)/shard_map/reshape | solution.py:121
  88.8 23.1 %all_to_all.16 = bf16[64,16,384]{2,1,0:T(8,128)(2,1)S(1)} all-to-all(bf16[64,16,384]{2,1,0:T(8,128)(2,1)} %reshape.81), channel_id=1, replica_groups=mesh['fs_0'=4,'fs_1'=4,'tp_0'=4,'tp_1'=2] {'fs_0','fs_1','tp_0'}, dimensions={0} | all-to-all | bytes 1572864 | tf_op jit(solution)/shard_map/all_to_all | solution.py:28
  114.1 5.7 %all-to-all-start.2 = ((f32[64,16,128]{2,1,0:T(8,128)}), f32[64,16,128]{2,1,0:T(8,128)}, u32[]{:S(2)}, u32[]{:S(2)}) async-start(f32[64,16,128]{2,1,0:T(8,128)} %bitcast.58), calls=%async_computation.2 | async-start | bytes 1048576 | tf_op jit(solution)/shard_map/all_to_all | solution.py:28
  121.7 1.5 copy.31
  123.2 8.8 %all-to-all-done.2 = f32[64,16,128]{2,1,0:T(8,128)} async-done(((f32[64,16,128]{2,1,0:T(8,128)}), f32[64,16,128]{2,1,0:T(8,128)}, u32[]{:S(2)}, u32[]{:S(2)}) %all-to-all-start.2) | async-done | bytes 524320 | tf_op jit(solution)/shard_map/all_to_all | solution.py:28
  132.1 2.0 %reshape.84 = f32[32,2,4,384]{3,2,1,0:T(4,128)} reshape(f32[64,12,128]{2,1,0:T(8,128)} %bitcast.50) | data formatting | bytes 786432 | tf_op jit(solution)/shard_map/reshape | solution.py:127
  134.0 1.8 %fusion.35 = (f32[32,1,4,384]{3,2,1,0:T(4,128)}, f32[32,1,4,384]{3,2,1,0:T(4,128)}) fusion(f32[32,2,4,384]{3,2,1,0:T(4,128)} %reshape.84), kind=kLoop, calls=%fused_computation.83 | loop fusion | bytes 786432 | tf_op jit(solution)/shard_map/slice | solution.py:129
  135.9 1.7 %reshape_squeeze.6 = f32[128,384]{1,0:T(8,128)} reshape(f32[32,1,4,384]{3,2,1,0:T(4,128)} %get-tuple-element.25) | data formatting | bytes 393216 | tf_op jit(solution)/shard_map/reshape;squeeze | solution.py:131
  137.5 1.6 %slice_reduce_fusion = f32[]{:T(128)} fusion(f32[64,16,128]{2,1,0:T(8,128)} %all-to-all-done.2), kind=kLoop, calls=%fused_computation.61 | loop fusion | flops 63 | bytes 260 | tf_op jit(solution)/shard_map/reduce_sum | solution.py:128
  139.2 2.3 %concatenate.40 = f32[136,384]{1,0:T(8,128)} pad(f32[128,384]{1,0:T(8,128)} %reshape_squeeze.6, f32[]{:T(128)} %slice_reduce_fusion), padding=0_8x0_0 | pad | bytes 405508 | tf_op jit(solution)/shard_map/concatenate | solution.py:130
  143.3 1.2 slice.161
  146.9 1.2 fusion.13
  148.2 1.3 fusion.29
  149.6 1.3 fusion.28
  150.9 1.3 fusion.18
  152.3 1.1 fusion.1
  154.5 1.2 fusion.3
  (65 shorter events, 18.8 us)
Async XLA Ops:
  44.1 13.7 %copy-start = (bf16[16,192,128]{2,1,0:T(8,128)(2,1)}, bf16[16,192,128]{2,1,0:T(8,128)(2,1)S(1)}, u32[]{:S(2)}) copy-start(bf16[16,192,128]{2,1,0:T(8,128)(2,1)S(1)} %slice.148) | copy-start | bytes 2359300
  44.1 2.4 %collective-permute-start = (bf16[16,192,128]{2,1,0:T(8,128)(2,1)S(1)}, bf16[16,192,128]{2,1,0:T(8,128)(2,1)S(1)}, u32[]{:S(2)}, u32[]{:S(2)}) collective-permute-start(bf16[16,192,128]{2,1,0:T(8,128)(2,1)S(1)} %slice.148), channel_id=1, source_target_pairs={{0,1},{1,0},{2,3},{3,2},{4,5},{5,4},{6,7},{7,6},{8,9},{9,8},{10,11... | collective-permute-start | bytes 2359304 | tf_op jit(solution)/shard_map/ppermute | solution.py:36
  46.5 0.9 copy-start.3
  73.4 2.6 %collective-permute-start.1 = (bf16[128,3072]{1,0:T(8,128)(2,1)}, bf16[128,3072]{1,0:T(8,128)(2,1)}, u32[]{:S(2)}, u32[]{:S(2)}) collective-permute-start(bf16[128,3072]{1,0:T(8,128)(2,1)} %pad_maximum_fusion), channel_id=1, source_target_pairs={{0,1},{1,0},{2,3},{3,2},{4,5},{5,4},{6,7},{7,6},{8,9},{9,8},{10,11... | collective-permute-start | bytes 2359304 | tf_op jit(solution)/shard_map/ppermute | solution.py:36
  73.5 4.9 %copy-start.5 = (f32[256,2048]{1,0:T(8,128)S(1)}, f32[256,2048]{1,0:T(8,128)}, u32[]{:S(2)}) copy-start(f32[256,2048]{1,0:T(8,128)} %fusion.4) | copy-start | bytes 6291460
  114.1 17.9 %all-to-all-start.2 = ((f32[64,16,128]{2,1,0:T(8,128)}), f32[64,16,128]{2,1,0:T(8,128)}, u32[]{:S(2)}, u32[]{:S(2)}) async-start(f32[64,16,128]{2,1,0:T(8,128)} %bitcast.58), calls=%async_computation.2 | async-start | bytes 1048576 | tf_op jit(solution)/shard_map/all_to_all | solution.py:28
  141.4 8.1 %copy-start.10 = (f32[16,256]{1,0:T(8,128)S(1)}, f32[16,256]{1,0:T(8,128)}, u32[]{:S(2)}) copy-start(f32[16,256]{1,0:T(8,128)} %param.22) | copy-start | bytes 49156
  141.5 1.8 %collective-permute-start.2 = (f32[136,384]{1,0:T(8,128)}, f32[136,384]{1,0:T(8,128)}, u32[]{:S(2)}, u32[]{:S(2)}) collective-permute-start(f32[136,384]{1,0:T(8,128)} %concatenate.40), channel_id=1, source_target_pairs={{0,1},{1,0},{2,3},{3,2},{4,5},{5,4},{6,7},{7,6},{8,9},{9,8},{10,11... | collective-permute-start | bytes 626696 | tf_op jit(solution)/shard_map/ppermute | solution.py:36
  145.8 2.3 %copy-start.6 = (f32[16,16,128]{2,1,0:T(8,128)S(1)}, f32[16,16,128]{2,1,0:T(8,128)}, u32[]{:S(2)}) copy-start(f32[16,16,128]{2,1,0:T(8,128)} %get-tuple-element.18) | copy-start | bytes 393220
  145.8 2.3 %copy-start.7 = (f32[16,16,128]{2,1,0:T(8,128)S(1)}, f32[16,16,128]{2,1,0:T(8,128)}, u32[]{:S(2)}) copy-start(f32[16,16,128]{2,1,0:T(8,128)} %get-tuple-element.19) | copy-start | bytes 393220
  146.9 5.4 %copy-start.1 = (bf16[16,64,256]{2,1,0:T(8,128)(2,1)S(1)}, bf16[16,64,256]{2,1,0:T(8,128)(2,1)}, u32[]{:S(2)}) copy-start(bf16[16,64,256]{2,1,0:T(8,128)(2,1)} %pad_maximum_fusion.2) | copy-start | bytes 1572868
  146.9 5.4 %copy-start.2 = (f32[16,2,64,128]{3,1,2,0:T(2,128)S(1)}, f32[16,2,64,128]{3,1,2,0:T(2,128)}, u32[]{:S(2)}) copy-start(f32[16,2,64,128]{3,1,2,0:T(2,128)} %copy.31) | copy-start | bytes 3145732
  152.3 1.2 copy-start.8
  153.4 1.1 copy-start.4
  154.5 1.3 copy-start.9

commit v2 on v1

v2 whole, which is shorter than its diff:
```python
import jax
import jax.numpy as jnp
from jax import lax
from jax.experimental import pallas as pl
from jax.experimental.pallas import tpu as pltpu
from jax.sharding import Mesh
from jax.sharding import PartitionSpec as P


D = 2048
DM = 1024
R = 256
FS = ("fs_0", "fs_1")
TP = ("tp_0", "tp_1")
CHIPS = ("fs_0", "fs_1", "tp_0")
CORE = "tp_1"
FS_TP = ("fs_0", "fs_1", "tp_0", "tp_1")
HALF = R // 2

momentum_decay = 0.9
square_decay = 0.95
adam_epsilon = 1e-08
update_scale = 0.25
learning_rate = 0.01

bf16 = jnp.bfloat16
f32 = jnp.float32

FACTOR_ROWS = 192
FIRST = (192, 224, 240)
SECOND = (208, 256, 272)
BLOCK_ROWS = 288
VALUE_W = 0
OUT_W = 128
WEIGHT_ROWS = 256


def exchange(tiles, axis):
    return lax.all_to_all(tiles, axis, split_axis=0, concat_axis=0, tiled=True)


def shifted(x, axis):
    out = [x]
    for d in (1, 2, 3):
        out.append(lax.ppermute(x, axis, [(i, (i + d) % 4) for i in range(4)]))
    return out


def near(x):
    return pltpu.with_memory_space_constraint(x, pltpu.VMEM)


def far(x):
    return pltpu.with_memory_space_constraint(x, pltpu.HBM)


def partner(x):
    return lax.ppermute(x, CORE, [(0, 1), (1, 0)])


def call(body, *args, **kwargs):
    def run(*operands):
        return call_of(body, *args, **kwargs)(*operands)

    return run


def call_of(body, out_shape, n_in, scratch=(), smem=1, n_far=0, limit=16, flops=0):
    vmem = pl.BlockSpec(memory_space=pltpu.VMEM)
    many = isinstance(out_shape, (tuple, list))
    return pl.pallas_call(
        body,
        out_shape=out_shape,
        in_specs=[pl.BlockSpec(memory_space=pltpu.SMEM)] * smem
        + [vmem] * n_in
        + [pl.BlockSpec(memory_space=pltpu.HBM)] * n_far,
        out_specs=[vmem] * len(out_shape) if many else vmem,
        scratch_shapes=list(scratch),
        compiler_params=pltpu.CompilerParams(vmem_limit_bytes=limit << 20),
        cost_estimate=pl.CostEstimate(flops=flops, bytes_accessed=0, transcendentals=0)
        if flops
        else None,
    )


def pack_body(at, vf, of, vw, ow, v1, v2, o1, o2, out, weights, block):
    half = pl.ds(pl.multiple_of(HALF * at[0], HALF), HALF)
    block[0:128] = vf[:, half]
    block[128:192] = of[:, half]
    block[192:208] = v1[...].astype(bf16)
    block[208:224] = v2[...].astype(bf16)
    block[224:240] = o1[:, :128].astype(bf16)
    block[240:256] = o1[:, 128:].astype(bf16)
    block[256:272] = o2[:, :128].astype(bf16)
    block[272:288] = o2[:, 128:].astype(bf16)
    for k in range(16):
        out[k] = block[...]
    weights[0:128] = vw[...].astype(bf16)
    weights[128:192] = ow[:, :128].astype(bf16)
    weights[192:256] = ow[:, 128:].astype(bf16)


def place_body(at, w0, w1, w2, w3, out):
    row = at[1]
    for dz, part in enumerate((w0, w1, w2, w3)):
        for dy in range(4):
            from_z = jnp.bitwise_and(row // 4 - dz, 3)
            from_y = jnp.bitwise_and(row - dy, 3)
            out[4 * from_z + from_y] = part[dy]


def join_factors(mine, other, fv, fo):
    for lanes, part in ((slice(0, 128), mine), (slice(128, 256), other)):
        for k in range(16):
            fv[128 * k : 128 * k + 128, lanes] = part[k, 0:128]
            fo[64 * k : 64 * k + 64, lanes] = part[k, 128:192]


def arrange(acc, first_row, core, out):
    low_rows = lax.broadcasted_iota(jnp.int32, (16, 8, 128), 1) < 4
    for h in range(2):
        column = jnp.bitwise_xor(core, h)
        for j in range(3):
            quads = []
            for x in range(4):
                if j == 0:
                    start = 256 * x + 128 * column
                else:
                    start = DM + 512 * x + 256 * column + 128 * (j - 1)
                lanes = pl.ds(pl.multiple_of(start, 128), 128)
                quads.append(acc[first_row : first_row + HALF, lanes].reshape(16, 8, 128))
            rolled = [pltpu.roll(q, 4, 1) for q in quads]
            low = [
                jnp.where(low_rows, quads[0], rolled[1]),
                jnp.where(low_rows, quads[2], rolled[3]),
            ]
            high = [
                jnp.where(low_rows, rolled[0], quads[1]),
                jnp.where(low_rows, rolled[2], quads[3]),
            ]
            lanes = slice(128 * j, 128 * j + 128)
            out[:, 2 * h, :, lanes] = jnp.concatenate(low, axis=1).astype(out.dtype)
            out[:, 2 * h + 1, :, lanes] = jnp.concatenate(high, axis=1).astype(out.dtype)


ACROSS = (((0,), (0,)), ((), ()))


def tokens_body(
    at, mine, other, x_far, c_far, h_far, o_far,
    kept, sent, fv, fo, acc, vb, ob, x, c, h, o, sems,
):
    step = x.shape[0] // 4

    def rows(i):
        return pl.ds(pl.multiple_of(i * step, step), step)

    def lanes(i):
        return pl.ds(pl.multiple_of(i * 512, 512), 512)

    def h_copy(i):
        return pltpu.make_async_copy(h_far.at[rows(i)], h.at[rows(i)], sems.at[i])

    def c_copy(i):
        return pltpu.make_async_copy(c_far.at[:, lanes(i)], c.at[:, lanes(i)], sems.at[4 + i])

    def o_copy(i):
        return pltpu.make_async_copy(o_far.at[:, lanes(i)], o.at[:, lanes(i)], sems.at[6 + i])

    def x_copy(i):
        return pltpu.make_async_copy(x_far.at[rows(i)], x.at[rows(i)], sems.at[10 + i])

    for i in range(4):
        h_copy(i).start()
    x_copy(0).start()
    join_factors(mine, other, fv, fo)

    def saved(i, carry):
        x_copy(i).wait()
        o_copy(i).start()
        vb[rows(i)] = jnp.dot(x[rows(i)], fv[...], preferred_element_type=f32).astype(bf16)
        return carry

    def hidden(i, carry):
        h_copy(i).wait()

        @pl.when(i < 3)
        def _():
            x_copy(i + 1).start()

        ob[rows(i)] = jnp.dot(h[rows(i)], fo[...], preferred_element_type=f32).astype(bf16)
        return carry

    def value_part(i, carry):
        c_copy(i).wait()
        acc[:, lanes(i)] = lax.dot_general(
            vb[...], c[:, lanes(i)], ACROSS, preferred_element_type=f32
        )
        return carry

    def out_part(i, carry):
        o_copy(i).wait()
        acc[:, pl.ds(pl.multiple_of(DM + i * 512, 512), 512)] = lax.dot_general(
            ob[...], o[:, lanes(i)], ACROSS, preferred_element_type=f32
        )
        return carry

    lax.fori_loop(0, 4, hidden, 0)
    c_copy(0).start()
    c_copy(1).start()
    lax.fori_loop(0, 4, saved, 0)
    lax.fori_loop(0, 2, value_part, 0)
    lax.fori_loop(0, 4, out_part, 0)
    arrange(acc, HALF, 1 - at[0], sent)
    arrange(acc, 0, at[0], kept)


def reply_body(tiles, out, own, stage):
    own[...] = jnp.sum(tiles[...].astype(f32), axis=0)
    squares = jnp.sum(own[...] * own[...])
    for x in range(4):
        for j in range(3):
            stage[x, 4 * j : 4 * j + 4] = own[4 * x : 4 * x + 4, 128 * j : 128 * j + 128]
        stage[x, 12:16] = jnp.full((4, 128), squares, f32)
    for k in range(16):
        out[4 * k : 4 * k + 4] = stage[...]


def sum_of_squares(back):
    return jnp.sum(back[:, :, 12:16]) * (1.0 / 512.0)


def hand_body(back, out):
    out[...] = back[:, 2:4]
    out[:, :, 12:16] = jnp.full((16, 2, 4, 128), sum_of_squares(back), f32)


def moments(first, second, scaled):
    new_first = momentum_decay * first + (1.0 - momentum_decay) * scaled
    new_second = square_decay * second + (1.0 - square_decay) * scaled * scaled
    return new_first, new_second


def finish_body(
    at, back, came, got, other, weights, vw, ow, v1, v2, o1, o2,
    vup, oup, nvw, now, vcopy, ocopy, nv1, nv2, no1, no2,
    low, fv, fo, ratios, vall, oall,
):
    core, row, start = at[0], at[1], at[2]
    total = sum_of_squares(back) + came[0, 0, 12, 0]
    root_mean = jnp.sqrt(jnp.full((8, 128), total, f32) / (R * (D + DM)))
    clip_factor = (1.0 / jnp.maximum(root_mean, 1.0))[0:1]

    low_rows = lax.broadcasted_iota(jnp.int32, (16, 8, 128), 1) < 4
    for half, part in ((0, back), (1, came)):
        shard = pl.ds(8 * jnp.bitwise_xor(core, half), 8)
        ranks = slice(HALF * half, HALF * half + HALF)
        a, b = part[:, 0], part[:, 1]
        joined = (
            jnp.where(low_rows, a[:, :8], pltpu.roll(b[:, :8], 4, 1)),
            jnp.where(low_rows, pltpu.roll(a[:, :8], 4, 1), b[:, :8]),
            jnp.where(low_rows, a[:, 8:], pltpu.roll(b[:, 8:], 4, 1)),
        )
        for j in range(3):
            scaled = joined[j].reshape(HALF, 128) * clip_factor
            low[ranks, 128 * j : 128 * j + 128] = scaled
            first = got[shard, FIRST[j] : FIRST[j] + 16].astype(f32).reshape(HALF, 128)
            second = got[shard, SECOND[j] : SECOND[j] + 16].astype(f32).reshape(HALF, 128)
            first, second = moments(first, second, scaled)
            ratio = first / (jnp.sqrt(second) + adam_epsilon)
            high = ratio.astype(bf16)
            rest = (ratio - high.astype(f32)).astype(bf16)
            at_high, at_rest = ((0, 128), (256, 512), (384, 640))[j]
            ratios[ranks, at_high : at_high + 128] = high
            ratios[ranks, at_rest : at_rest + 128] = rest

    own = pl.ds(pl.multiple_of(start, 16), 16)
    nv1[...], nv2[...] = moments(v1[...], v2[...], low[own, 0:128])
    no1[...], no2[...] = moments(o1[...], o2[...], low[own, 128:384])

    join_factors(got, other, fv, fo)
    for k in range(4):
        rows = slice(512 * k, 512 * k + 512)
        both = jnp.dot(fv[rows], ratios[:, 0:256], preferred_element_type=f32)
        update = update_scale * (both[:, :128] + both[:, 128:])
        vall[rows] = update
        weight = weights[4 * k : 4 * k + 4, VALUE_W : VALUE_W + 128].astype(f32).reshape(512, 128)
        vcopy[rows] = (weight - learning_rate * update).astype(bf16)
    for k in range(2):
        rows = slice(512 * k, 512 * k + 512)
        both = jnp.dot(fo[rows], ratios[:, 256:768], preferred_element_type=f32)
        update = update_scale * (both[:, :256] + both[:, 256:])
        oall[rows] = update
        for side in range(2):
            lanes = slice(128 * side, 128 * side + 128)
            at_w = OUT_W + 64 * side
            weight = weights[8 * k : 8 * k + 8, at_w : at_w + 64].astype(f32).reshape(512, 128)
            ocopy[rows, lanes] = (weight - learning_rate * update[:, lanes]).astype(bf16)

    update = vall[pl.ds(pl.multiple_of(128 * row, 128), 128)]
    vup[...] = update
    nvw[...] = vw[...] - learning_rate * update
    update = oall[pl.ds(pl.multiple_of(64 * row, 64), 64)]
    oup[...] = update
    now[...] = ow[...] - learning_rate * update


def shards(x, c, h, o, vf, of, vw, ow, v1, v2, o1, o2):
    core = lax.axis_index(CORE)
    row = lax.axis_index(FS)
    start = HALF * jnp.bitwise_xor(row // 8, core) + 16 * (row % 8)
    at = jnp.stack([core, row, start]).astype(jnp.int32)

    blocks, weights = call(
        pack_body,
        (pltpu.VMEM((16, BLOCK_ROWS, 128), bf16), pltpu.VMEM((WEIGHT_ROWS, 128), bf16)),
        8,
        [pltpu.VMEM((BLOCK_ROWS, 128), bf16)],
    )(at, *map(far, (vf, of, vw, ow, v1, v2, o1, o2)))
    got = exchange(blocks, FS)
    got, weights = lax.optimization_barrier((got, weights))
    other = partner(got[:, :FACTOR_ROWS])
    along_y = jnp.stack(shifted(weights, "fs_1"))
    parts = shifted(along_y, "fs_0")

    kept, sent = call(
        tokens_body,
        (pltpu.VMEM((16, 4, 16, 384), f32), pltpu.VMEM((16, 4, 16, 384), bf16)),
        2,
        [
            pltpu.VMEM((D, R), bf16),
            pltpu.VMEM((DM, R), bf16),
            pltpu.VMEM((R, D + DM), f32),
            pltpu.VMEM((x.shape[0], R), bf16),
            pltpu.VMEM((x.shape[0], R), bf16),
            pltpu.VMEM(x.shape, bf16),
            pltpu.VMEM(c.shape, bf16),
            pltpu.VMEM(h.shape, bf16),
            pltpu.VMEM(o.shape, bf16),
            pltpu.SemaphoreType.DMA((14,)),
        ],
        n_far=4,
        limit=36,
        flops=12 * x.shape[0] * D * R,
    )(at, near(got), near(other), far(x), far(c), far(h), far(o))
    came = partner(sent)
    tiles = (kept + came.astype(f32)).astype(bf16)
    tiles = exchange(tiles.reshape(64, 16, 384), CHIPS)
    replies = call(
        reply_body,
        pltpu.VMEM((64, 16, 128), f32),
        1,
        [pltpu.VMEM((16, 384), f32), pltpu.VMEM((4, 16, 128), f32)],
        smem=0,
    )(near(tiles))
    back = exchange(replies, CHIPS).reshape(16, 4, 16, 128)
    back = near(back)
    weights = call(place_body, pltpu.VMEM((16, WEIGHT_ROWS, 128), bf16), 4)(
        at, *[near(p) for p in parts]
    )
    came = partner(call(hand_body, pltpu.VMEM((16, 2, 16, 128), f32), 1, smem=0)(back))

    def like(a, dtype=f32):
        return jax.ShapeDtypeStruct(a.shape, dtype)

    return call(
        finish_body,
        (
            like(vw),
            like(ow),
            like(vw),
            like(ow),
            jax.ShapeDtypeStruct((D, 128), bf16),
            jax.ShapeDtypeStruct((DM, 256), bf16),
            like(v1),
            like(v2),
            like(o1),
            like(o2),
        ),
        11,
        [
            pltpu.VMEM((R, 384), f32),
            pltpu.VMEM((D, R), bf16),
            pltpu.VMEM((DM, R), bf16),
            pltpu.VMEM((R, 768), bf16),
            pltpu.VMEM((D, 128), f32),
            pltpu.VMEM((DM, 256), f32),
        ],
    )(at, back, near(came), near(got), near(other), near(weights), vw, ow, v1, v2, o1, o2)


def solution(mesh):
    torus = Mesh(mesh.devices.reshape(4, 4, 4, 2), FS_TP)
    return jax.shard_map(
        shards,
        mesh=torus,
        in_specs=(P(FS_TP, None),) * 4 + (P(FS, None),) * 2 + (P(FS, TP),) * 6,
        out_specs=(P(FS, TP),) * 4 + (P(None, TP),) * 2 + (P(FS, TP),) * 4,
        check_vma=False,
    )
```

time: 159 us -> 106 us (0.67); the launches traced: 156 us -> 105 us
  local copies, waits for them, and re-layouts: 28 us -> 0.11 us
  matrix products: 22.8 us -> 0 us
  other arithmetic: 23 us -> 0.32 us
  Pallas kernels: 0 us -> 17.9 us
  blocking collectives: 60.8 us -> 49.4 us
  starting transfers between devices: 5.89 us -> 15.5 us
  waiting for transfers between devices: 13.7 us -> 21.4 us
    dot_general x6 -> x0, matrix products: 22.8 us -> none  [the longest x1 9.62 us: shards(): jnp.einsum('tr,tc->rc', out_basis, out_cotangent, preferred_element_type=...]
    pallas_call x0 -> x6, Pallas kernels: none -> 17.9 us  [run(): return call_of(body, *args, **kwargs)(*operands)]
    ppermute x0 -> x6, waiting for transfers between devices: none -> 17 us  [shifted(): out.append(lax.ppermute(x, axis, [(i, (i + d) % 4) for i in range(4)]))]
    all_to_all x2, blocking collectives: 60.8 us -> 49.4 us  [exchange(): return lax.all_to_all(tiles, axis, split_axis=0, concat_axis=0, tiled=True)]
    ppermute x0 -> x6, starting transfers between devices: none -> 10.5 us  [shifted(): out.append(lax.ppermute(x, axis, [(i, (i + d) % 4) for i in range(4)]))]
    reshape x7 -> x0, local copies, waits for them, and re-layouts: 9.67 us -> none  [the longest x4 5.42 us: columns(): a = a.reshape(32, 4, 4, 2, width)]
    all_to_all x1, waiting for transfers between devices: 8.84 us -> 0.01 us  [exchange(): return lax.all_to_all(tiles, axis, split_axis=0, concat_axis=0, tiled=True)]
    slice x9 -> x1, local copies, waits for them, and re-layouts: 8.1 us -> 0.07 us  [shards(): other = partner(got[:, :FACTOR_ROWS])]
  transfers between devices with their start and end apart: 4 -> 10, of which waited for: 4 -> 7; matrix products, arithmetic and copies ran while one was open for 3% -> 0% of each run, Pallas kernels for 0% -> 1%
where the time goes in v2:
time: 106 us; the launch traced here: 105 us
  blocking collectives  49.4 us (47%)
  waiting for transfers between devices  21.4 us (20%)
  Pallas kernels  17.9 us (17%)
  starting transfers between devices  15.5 us (15%)
    all_to_all x2, blocking collectives, exchange(): return lax.all_to_all(tiles, axis, split_axis=0, concat_axis=0, tiled=True)  49.4 us
    pallas_call x6, Pallas kernels, run(): return call_of(body, *args, **kwargs)(*operands)  17.9 us
    ppermute x6, waiting for transfers between devices, shifted(): out.append(lax.ppermute(x, axis, [(i, (i + d) % 4) for i in range(4)]))  17 us
    ppermute x6, starting transfers between devices, shifted(): out.append(lax.ppermute(x, axis, [(i, (i + d) % 4) for i in range(4)]))  10.5 us
    all_to_all x1, starting transfers between devices, exchange(): return lax.all_to_all(tiles, axis, split_axis=0, concat_axis=0, tiled=True)  4.64 us
    ppermute x3, waiting for transfers between devices, partner(): return lax.ppermute(x, CORE, [(0, 1), (1, 0)])  4.42 us
  transfers between devices with their start and end apart: 10, of which 7 were waited for; matrix products, arithmetic and copies ran while one was open for 0% of the time, Pallas kernels for 1%

profile of v2, /device:TPU:0, one launch (start us, length us, event | category | flops | bytes accessed | tf_op | source)
XLA Modules:
  0.0 105.4 jit_solution(220372857523134600)
XLA Ops:
  0.7 0.1 pad_add_fusion.at
  0.7 1.1 %shard_map.195 = (bf16[16,288,128]{2,1,0:T(8,128)(2,1)S(1)}, bf16[256,128]{1,0:T(8,128)(2,1)S(1)}) custom-call(s32[3]{0:T(128)S(1)} %pad_add_fusion.at, bf16[128,256]{1,0:T(8,128)(2,1)} %vf.1, bf16[64,256]{1,0:T(8,128)(2,1)} %of.1, f32[128,128]{1,0:T(8,128)} %vw.3, f32[64,256]{1,0:T(8,128)} %ow.3, f32[16,128]{1,0:T(8,128)} %v1.3, f32[16,128]{1,0:T(8,128)} %v2.3, ...), custom_call_target="tpu_custom_call" | custom-call | tf_op jit(solution)/shard_map/pallas_call | solution.py:63
  1.9 26.5 %all_to_all.15.mine.got = bf16[16,288,128]{2,1,0:T(8,128)(2,1)S(1)} all-to-all(bf16[16,288,128]{2,1,0:T(8,128)(2,1)S(1)} %get-tuple-element.16), channel_id=1, replica_groups=mesh['fs_0'=4,'fs_1'=4,'tp_0'=4,'tp_1'=2] {'fs_0','fs_1'}, dimensions={0} | all-to-all | bytes 2359296 | tf_op jit(solution)/shard_map/all_to_all | solution.py:39
  28.4 0.1 slice.3
  28.5 0.1 collective-permute-start
  28.6 2.3 %collective-permute-done.other = bf16[16,192,128]{2,1,0:T(8,128)(2,1)S(1)} collective-permute-done((bf16[16,192,128]{2,1,0:T(8,128)(2,1)S(1)}, bf16[16,192,128]{2,1,0:T(8,128)(2,1)S(1)}, u32[]{:S(2)}, u32[]{:S(2)}) %collective-permute-start) | collective-permute-done | bytes 786464 | tf_op jit(solution)/shard_map/ppermute | solution.py:58
  30.8 11.5 %shard_map.196 = (f32[16,4,16,384]{3,2,1,0:T(8,128)S(1)}, bf16[16,4,16,384]{3,2,1,0:T(8,128)(2,1)S(1)}) custom-call(s32[3]{0:T(128)S(1)} %pad_add_fusion.at, bf16[16,288,128]{2,1,0:T(8,128)(2,1)S(1)} %all_to_all.15.mine.got, bf16[16,192,128]{2,1,0:T(8,128)(2,1)S(1)} %collective-permute-done.other, bf16[2048,2048]{1,0:T(8,128)(2,1)} %x_far.1, ...), custom_call_target="tpu_custom_call" | custom-call | flops 12884901888 | tf_op jit(solution)/shard_map/pallas_call | solution.py:63
  42.3 0.2 collective-permute-start.1
  42.5 2.1 %collective-permute-done.1 = bf16[16,4,16,384]{3,2,1,0:T(8,128)(2,1)S(1)} collective-permute-done((bf16[16,4,16,384]{3,2,1,0:T(8,128)(2,1)S(1)}, bf16[16,4,16,384]{3,2,1,0:T(8,128)(2,1)S(1)}, u32[]{:S(2)}, u32[]{:S(2)}) %collective-permute-start.1) | collective-permute-done | bytes 786464 | tf_op jit(solution)/shard_map/ppermute | solution.py:58
  44.7 0.2 add_convert_fusion
  44.9 22.9 %all_to_all.16.tiles = bf16[64,16,384]{2,1,0:T(8,128)(2,1)S(1)} all-to-all(bf16[64,16,384]{2,1,0:T(8,128)(2,1)S(1)} %bitcast.12), channel_id=1, replica_groups=mesh['fs_0'=4,'fs_1'=4,'tp_0'=4,'tp_1'=2] {'fs_0','fs_1','tp_0'}, dimensions={0} | all-to-all | bytes 1572864 | tf_op jit(solution)/shard_map/all_to_all | solution.py:39
  67.8 1.1 %shard_map.197 = f32[64,16,128]{2,1,0:T(8,128)} custom-call(bf16[64,16,384]{2,1,0:T(8,128)(2,1)S(1)} %all_to_all.16.tiles), custom_call_target="tpu_custom_call" | custom-call | tf_op jit(solution)/shard_map/pallas_call | solution.py:63
  68.9 4.6 %all-to-all-start.2 = ((f32[64,16,128]{2,1,0:T(8,128)}), f32[64,16,128]{2,1,0:T(8,128)S(1)}, u32[]{:S(2)}, u32[]{:S(2)}) async-start(f32[64,16,128]{2,1,0:T(8,128)} %shard_map.197), calls=%async_computation.2 | async-start | bytes 1048576 | tf_op jit(solution)/shard_map/all_to_all | solution.py:39
  73.5 2.9 %collective-permute-start.5 = (bf16[256,128]{1,0:T(8,128)(2,1)S(1)}, bf16[256,128]{1,0:T(8,128)(2,1)S(1)}, u32[]{:S(2)}, u32[]{:S(2)}) collective-permute-start(bf16[256,128]{1,0:T(8,128)(2,1)S(1)} %get-tuple-element.21), channel_id=1, source_target_pairs={{0,24},{8,0},{16,8},{24,16},{1,25},{9,1},{17,9},{25,17},{2,26},{10... | collective-permute-start | bytes 196616 | tf_op jit(solution)/shard_map/ppermute | solution.py:45
  76.4 0.9 collective-permute-start.4
  77.2 0.9 collective-permute-start.3
  78.1 4.2 %collective-permute-done.5 = bf16[256,128]{1,0:T(8,128)(2,1)S(1)} collective-permute-done((bf16[256,128]{1,0:T(8,128)(2,1)S(1)}, bf16[256,128]{1,0:T(8,128)(2,1)S(1)}, u32[]{:S(2)}, u32[]{:S(2)}) %collective-permute-start.5) | collective-permute-done | bytes 65568 | tf_op jit(solution)/shard_map/ppermute | solution.py:45
  82.3 2.1 %collective-permute-done.4 = bf16[256,128]{1,0:T(8,128)(2,1)S(1)} collective-permute-done((bf16[256,128]{1,0:T(8,128)(2,1)S(1)}, bf16[256,128]{1,0:T(8,128)(2,1)S(1)}, u32[]{:S(2)}, u32[]{:S(2)}) %collective-permute-start.4) | collective-permute-done | bytes 65568 | tf_op jit(solution)/shard_map/ppermute | solution.py:45
  84.4 0.6 collective-permute-done.3
  85.0 0.0 copy-start
  85.0 0.0 copy-start.1
  85.0 0.0 copy-start.3
  85.1 0.0 copy-start.4
  85.1 1.6 %collective-permute-start.6 = (bf16[4,256,128]{2,1,0:T(8,128)(2,1)S(1)}, bf16[4,256,128]{2,1,0:T(8,128)(2,1)S(1)}, u32[]{:S(2)}, u32[]{:S(2)}) collective-permute-start(bf16[4,256,128]{2,1,0:T(8,128)(2,1)S(1)} %pad_maximum_fusion.w0), channel_id=1, source_target_pairs={{0,32},{32,64},{64,96},{96,0},{1,33},{33,65},{65,97},{97,1},{2,34}... | collective-permute-start | bytes 786440 | tf_op jit(solution)/shard_map/ppermute | solution.py:45
  86.7 2.9 %collective-permute-start.7 = (bf16[4,256,128]{2,1,0:T(8,128)(2,1)S(1)}, bf16[4,256,128]{2,1,0:T(8,128)(2,1)S(1)}, u32[]{:S(2)}, u32[]{:S(2)}) collective-permute-start(bf16[4,256,128]{2,1,0:T(8,128)(2,1)S(1)} %pad_maximum_fusion.w0), channel_id=1, source_target_pairs={{0,64},{32,96},{64,0},{96,32},{1,65},{33,97},{65,1},{97,33},{2,66}... | collective-permute-start | bytes 786440 | tf_op jit(solution)/shard_map/ppermute | solution.py:45
  89.6 1.4 %collective-permute-start.8 = (bf16[4,256,128]{2,1,0:T(8,128)(2,1)S(1)}, bf16[4,256,128]{2,1,0:T(8,128)(2,1)}, u32[]{:S(2)}, u32[]{:S(2)}) collective-permute-start(bf16[4,256,128]{2,1,0:T(8,128)(2,1)S(1)} %pad_maximum_fusion.w0), channel_id=1, source_target_pairs={{0,96},{32,0},{64,32},{96,64},{1,97},{33,1},{65,33},{97,65},{2,98}... | collective-permute-start | bytes 786440 | tf_op jit(solution)/shard_map/ppermute | solution.py:45
  91.0 0.2 shard_map.198
  91.2 0.1 collective-permute-start.2
  91.3 3.3 %collective-permute-done.6.w1 = bf16[4,256,128]{2,1,0:T(8,128)(2,1)S(1)} collective-permute-done((bf16[4,256,128]{2,1,0:T(8,128)(2,1)S(1)}, bf16[4,256,128]{2,1,0:T(8,128)(2,1)S(1)}, u32[]{:S(2)}, u32[]{:S(2)}) %collective-permute-start.6) | collective-permute-done | bytes 262176 | tf_op jit(solution)/shard_map/ppermute | solution.py:45
  94.6 6.8 %collective-permute-done.7.w2 = bf16[4,256,128]{2,1,0:T(8,128)(2,1)S(1)} collective-permute-done((bf16[4,256,128]{2,1,0:T(8,128)(2,1)S(1)}, bf16[4,256,128]{2,1,0:T(8,128)(2,1)S(1)}, u32[]{:S(2)}, u32[]{:S(2)}) %collective-permute-start.7) | collective-permute-done | bytes 262176 | tf_op jit(solution)/shard_map/ppermute | solution.py:45
  101.4 1.0 shard_map.199.weights
  102.5 2.9 %shard_map.200 = (f32[128,128]{1,0:T(8,128)}, f32[64,256]{1,0:T(8,128)}, f32[128,128]{1,0:T(8,128)}, f32[64,256]{1,0:T(8,128)}, bf16[2048,128]{1,0:T(8,128)(2,1)...) custom-call(s32[3]{0:T(128)S(1)} %pad_add_fusion.at, ...), custom_call_target="tpu_custom_call" | custom-call | tf_op jit(solution)/shard_map/pallas_call | solution.py:63
  (12 shorter events, 0.1 us)
Async XLA Ops:
  28.5 2.4 %collective-permute-start = (bf16[16,192,128]{2,1,0:T(8,128)(2,1)S(1)}, bf16[16,192,128]{2,1,0:T(8,128)(2,1)S(1)}, u32[]{:S(2)}, u32[]{:S(2)}) collective-permute-start(bf16[16,192,128]{2,1,0:T(8,128)(2,1)S(1)} %slice.3), channel_id=1, source_target_pairs={{0,1},{1,0},{2,3},{3,2},{4,5},{5,4},{6,7},{7,6},{8,9},{9,8},{10,11... | collective-permute-start | bytes 2359304 | tf_op jit(solution)/shard_map/ppermute | solution.py:58
  42.3 2.4 %collective-permute-start.1 = (bf16[16,4,16,384]{3,2,1,0:T(8,128)(2,1)S(1)}, bf16[16,4,16,384]{3,2,1,0:T(8,128)(2,1)S(1)}, u32[]{:S(2)}, u32[]{:S(2)}) collective-permute-start(bf16[16,4,16,384]{3,2,1,0:T(8,128)(2,1)S(1)} %get-tuple-element.20), channel_id=1, source_target_pairs={{0,1},{1,0},{2,3},{3,2},{4,5},{5,4},{6,7},{7,6},{8,9},{9,8},{10,11... | collective-permute-start | bytes 2359304 | tf_op jit(solution)/shard_map/ppermute | solution.py:58
  68.9 22.1 %all-to-all-start.2 = ((f32[64,16,128]{2,1,0:T(8,128)}), f32[64,16,128]{2,1,0:T(8,128)S(1)}, u32[]{:S(2)}, u32[]{:S(2)}) async-start(f32[64,16,128]{2,1,0:T(8,128)} %shard_map.197), calls=%async_computation.2 | async-start | bytes 1048576 | tf_op jit(solution)/shard_map/all_to_all | solution.py:39
  73.5 8.8 %collective-permute-start.5 = (bf16[256,128]{1,0:T(8,128)(2,1)S(1)}, bf16[256,128]{1,0:T(8,128)(2,1)S(1)}, u32[]{:S(2)}, u32[]{:S(2)}) collective-permute-start(bf16[256,128]{1,0:T(8,128)(2,1)S(1)} %get-tuple-element.21), channel_id=1, source_target_pairs={{0,24},{8,0},{16,8},{24,16},{1,25},{9,1},{17,9},{25,17},{2,26},{10... | collective-permute-start | bytes 196616 | tf_op jit(solution)/shard_map/ppermute | solution.py:45
  76.4 8.0 %collective-permute-start.4 = (bf16[256,128]{1,0:T(8,128)(2,1)S(1)}, bf16[256,128]{1,0:T(8,128)(2,1)S(1)}, u32[]{:S(2)}, u32[]{:S(2)}) collective-permute-start(bf16[256,128]{1,0:T(8,128)(2,1)S(1)} %get-tuple-element.21), channel_id=1, source_target_pairs={{0,16},{8,24},{16,0},{24,8},{1,17},{9,25},{17,1},{25,9},{2,18},{10... | collective-permute-start | bytes 196616 | tf_op jit(solution)/shard_map/ppermute | solution.py:45
  77.2 7.8 %collective-permute-start.3 = (bf16[256,128]{1,0:T(8,128)(2,1)S(1)}, bf16[256,128]{1,0:T(8,128)(2,1)S(1)}, u32[]{:S(2)}, u32[]{:S(2)}) collective-permute-start(bf16[256,128]{1,0:T(8,128)(2,1)S(1)} %get-tuple-element.21), channel_id=1, source_target_pairs={{0,8},{8,16},{16,24},{24,0},{1,9},{9,17},{17,25},{25,1},{2,10},{10... | collective-permute-start | bytes 196616 | tf_op jit(solution)/shard_map/ppermute | solution.py:45
  85.0 17.4 %copy-start = (f32[128,128]{1,0:T(8,128)S(1)}, f32[128,128]{1,0:T(8,128)}, u32[]{:S(2)}) copy-start(f32[128,128]{1,0:T(8,128)} %vw.3) | copy-start | bytes 196612
  85.0 17.4 %copy-start.1 = (f32[64,256]{1,0:T(8,128)S(1)}, f32[64,256]{1,0:T(8,128)}, u32[]{:S(2)}) copy-start(f32[64,256]{1,0:T(8,128)} %ow.3) | copy-start | bytes 196612
  85.0 17.4 %copy-start.2 = (f32[16,256]{1,0:T(8,128)S(1)}, f32[16,256]{1,0:T(8,128)}, u32[]{:S(2)}) copy-start(f32[16,256]{1,0:T(8,128)} %o1.3) | copy-start | bytes 49156
  85.0 17.4 %copy-start.3 = (f32[16,256]{1,0:T(8,128)S(1)}, f32[16,256]{1,0:T(8,128)}, u32[]{:S(2)}) copy-start(f32[16,256]{1,0:T(8,128)} %o2.3) | copy-start | bytes 49156
  85.1 17.4 %copy-start.4 = (f32[16,128]{1,0:T(8,128)S(1)}, f32[16,128]{1,0:T(8,128)}, u32[]{:S(2)}) copy-start(f32[16,128]{1,0:T(8,128)} %v1.3) | copy-start | bytes 24580
  85.1 17.4 %copy-start.5 = (f32[16,128]{1,0:T(8,128)S(1)}, f32[16,128]{1,0:T(8,128)}, u32[]{:S(2)}) copy-start(f32[16,128]{1,0:T(8,128)} %v2.3) | copy-start | bytes 24580
  85.1 9.5 %collective-permute-start.6 = (bf16[4,256,128]{2,1,0:T(8,128)(2,1)S(1)}, bf16[4,256,128]{2,1,0:T(8,128)(2,1)S(1)}, u32[]{:S(2)}, u32[]{:S(2)}) collective-permute-start(bf16[4,256,128]{2,1,0:T(8,128)(2,1)S(1)} %pad_maximum_fusion.w0), channel_id=1, source_target_pairs={{0,32},{32,64},{64,96},{96,0},{1,33},{33,65},{65,97},{97,1},{2,34}... | collective-permute-start | bytes 786440 | tf_op jit(solution)/shard_map/ppermute | solution.py:45
  86.7 14.6 %collective-permute-start.7 = (bf16[4,256,128]{2,1,0:T(8,128)(2,1)S(1)}, bf16[4,256,128]{2,1,0:T(8,128)(2,1)S(1)}, u32[]{:S(2)}, u32[]{:S(2)}) collective-permute-start(bf16[4,256,128]{2,1,0:T(8,128)(2,1)S(1)} %pad_maximum_fusion.w0), channel_id=1, source_target_pairs={{0,64},{32,96},{64,0},{96,32},{1,65},{33,97},{65,1},{97,33},{2,66}... | collective-permute-start | bytes 786440 | tf_op jit(solution)/shard_map/ppermute | solution.py:45
  89.6 11.7 %collective-permute-start.8 = (bf16[4,256,128]{2,1,0:T(8,128)(2,1)S(1)}, bf16[4,256,128]{2,1,0:T(8,128)(2,1)}, u32[]{:S(2)}, u32[]{:S(2)}) collective-permute-start(bf16[4,256,128]{2,1,0:T(8,128)(2,1)S(1)} %pad_maximum_fusion.w0), channel_id=1, source_target_pairs={{0,96},{32,0},{64,32},{96,64},{1,97},{33,1},{65,33},{97,65},{2,98}... | collective-permute-start | bytes 786440 | tf_op jit(solution)/shard_map/ppermute | solution.py:45
  91.2 11.2 %collective-permute-start.2 = (f32[16,2,16,128]{3,2,1,0:T(8,128)S(1)}, f32[16,2,16,128]{3,2,1,0:T(8,128)S(1)}, u32[]{:S(2)}, u32[]{:S(2)}) collective-permute-start(f32[16,2,16,128]{3,2,1,0:T(8,128)S(1)} %shard_map.198), channel_id=1, source_target_pairs={{0,1},{1,0},{2,3},{3,2},{4,5},{5,4},{6,7},{7,6},{8,9},{9,8},{10,11... | collective-permute-start | bytes 786440 | tf_op jit(solution)/shard_map/ppermute | solution.py:58

commit v3 on v2

--- a/solution.py
+++ b/solution.py
@@ -26,24 +26,20 @@
 bf16 = jnp.bfloat16
 f32 = jnp.float32
 
-FACTOR_ROWS = 192
-FIRST = (192, 224, 240)
-SECOND = (208, 256, 272)
-BLOCK_ROWS = 288
+BLOCK_ROWS = 192
 VALUE_W = 0
 OUT_W = 128
-WEIGHT_ROWS = 256
+FIRST = (256, 288, 304)
+SECOND = (272, 320, 336)
+STATE_ROWS = 352
 
 
 def exchange(tiles, axis):
     return lax.all_to_all(tiles, axis, split_axis=0, concat_axis=0, tiled=True)
 
 
-def shifted(x, axis):
-    out = [x]
-    for d in (1, 2, 3):
-        out.append(lax.ppermute(x, axis, [(i, (i + d) % 4) for i in range(4)]))
-    return out
+def shift(x, axis, d):
+    return lax.ppermute(x, axis, [(i, (i + d) % 4) for i in range(4)])
 
 
 def near(x):
@@ -83,30 +79,34 @@
     )
 
 
-def pack_body(at, vf, of, vw, ow, v1, v2, o1, o2, out, weights, block):
+def pack_body(at, vf, of, vw, ow, v1, v2, o1, o2, out, state, block):
     half = pl.ds(pl.multiple_of(HALF * at[0], HALF), HALF)
     block[0:128] = vf[:, half]
     block[128:192] = of[:, half]
-    block[192:208] = v1[...].astype(bf16)
-    block[208:224] = v2[...].astype(bf16)
-    block[224:240] = o1[:, :128].astype(bf16)
-    block[240:256] = o1[:, 128:].astype(bf16)
-    block[256:272] = o2[:, :128].astype(bf16)
-    block[272:288] = o2[:, 128:].astype(bf16)
     for k in range(16):
         out[k] = block[...]
-    weights[0:128] = vw[...].astype(bf16)
-    weights[128:192] = ow[:, :128].astype(bf16)
-    weights[192:256] = ow[:, 128:].astype(bf16)
-
-
-def place_body(at, w0, w1, w2, w3, out):
+    state[0:128] = vw[...].astype(bf16)
+    state[128:192] = ow[:, :128].astype(bf16)
+    state[192:256] = ow[:, 128:].astype(bf16)
+    state[256:272] = v1[...].astype(bf16)
+    state[272:288] = v2[...].astype(bf16)
+    state[288:304] = o1[:, :128].astype(bf16)
+    state[304:320] = o1[:, 128:].astype(bf16)
+    state[320:336] = o2[:, :128].astype(bf16)
+    state[336:352] = o2[:, 128:].astype(bf16)
+
+
+def place_body(at, w0, w1, up, down, w3, out):
     row = at[1]
-    for dz, part in enumerate((w0, w1, w2, w3)):
+    for dz in range(4):
         for dy in range(4):
             from_z = jnp.bitwise_and(row // 4 - dz, 3)
             from_y = jnp.bitwise_and(row - dy, 3)
-            out[4 * from_z + from_y] = part[dy]
+            if dz == 2:
+                part = up[dy] if dy < 2 else down[dy - 2]
+            else:
+                part = (w0, w1, None, w3)[dz][dy]
+            out[4 * from_z + from_y] = part
 
 
 def join_factors(mine, other, fv, fo):
@@ -191,17 +191,19 @@
         ob[rows(i)] = jnp.dot(h[rows(i)], fo[...], preferred_element_type=f32).astype(bf16)
         return carry
 
-    def value_part(i, carry):
-        c_copy(i).wait()
-        acc[:, lanes(i)] = lax.dot_general(
-            vb[...], c[:, lanes(i)], ACROSS, preferred_element_type=f32
-        )
+    def value_part(carry):
+        c_copy(0).wait()
+        c_copy(1).wait()
+        acc[:, :DM] = lax.dot_general(vb[...], c[...], ACROSS, preferred_element_type=f32)
         return carry
 
     def out_part(i, carry):
-        o_copy(i).wait()
-        acc[:, pl.ds(pl.multiple_of(DM + i * 512, 512), 512)] = lax.dot_general(
-            ob[...], o[:, lanes(i)], ACROSS, preferred_element_type=f32
+        o_copy(2 * i).wait()
+        o_copy(2 * i + 1).wait()
+        at_in = pl.ds(pl.multiple_of(i * 1024, 1024), 1024)
+        at_out = pl.ds(pl.multiple_of(DM + i * 1024, 1024), 1024)
+        acc[:, at_out] = lax.dot_general(
+            ob[...], o[:, at_in], ACROSS, preferred_element_type=f32
         )
         return carry
 
@@ -209,10 +211,15 @@
     c_copy(0).start()
     c_copy(1).start()
     lax.fori_loop(0, 4, saved, 0)
-    lax.fori_loop(0, 2, value_part, 0)
-    lax.fori_loop(0, 4, out_part, 0)
+    value_part(0)
+    lax.fori_loop(0, 2, out_part, 0)
     arrange(acc, HALF, 1 - at[0], sent)
     arrange(acc, 0, at[0], kept)
+
+
+def halves_body(replies, before, after, up, down):
+    up[...] = before[0:2]
+    down[...] = after[2:4]
 
 
 def reply_body(tiles, out, own, stage):
@@ -242,9 +249,9 @@
 
 
 def finish_body(
-    at, back, came, got, other, weights, vw, ow, v1, v2, o1, o2,
+    at, back, came, fv, fo, weights, vw, ow, v1, v2, o1, o2,
     vup, oup, nvw, now, vcopy, ocopy, nv1, nv2, no1, no2,
-    low, fv, fo, ratios, vall, oall,
+    low, ratios, vall, oall,
 ):
     core, row, start = at[0], at[1], at[2]
     total = sum_of_squares(back) + came[0, 0, 12, 0]
@@ -264,8 +271,8 @@
         for j in range(3):
             scaled = joined[j].reshape(HALF, 128) * clip_factor
             low[ranks, 128 * j : 128 * j + 128] = scaled
-            first = got[shard, FIRST[j] : FIRST[j] + 16].astype(f32).reshape(HALF, 128)
-            second = got[shard, SECOND[j] : SECOND[j] + 16].astype(f32).reshape(HALF, 128)
+            first = weights[shard, FIRST[j] : FIRST[j] + 16].astype(f32).reshape(HALF, 128)
+            second = weights[shard, SECOND[j] : SECOND[j] + 16].astype(f32).reshape(HALF, 128)
             first, second = moments(first, second, scaled)
             ratio = first / (jnp.sqrt(second) + adam_epsilon)
             high = ratio.astype(bf16)
@@ -278,7 +285,6 @@
     nv1[...], nv2[...] = moments(v1[...], v2[...], low[own, 0:128])
     no1[...], no2[...] = moments(o1[...], o2[...], low[own, 128:384])
 
-    join_factors(got, other, fv, fo)
     for k in range(4):
         rows = slice(512 * k, 512 * k + 512)
         both = jnp.dot(fv[rows], ratios[:, 0:256], preferred_element_type=f32)
@@ -313,23 +319,27 @@
 
     blocks, weights = call(
         pack_body,
-        (pltpu.VMEM((16, BLOCK_ROWS, 128), bf16), pltpu.VMEM((WEIGHT_ROWS, 128), bf16)),
+        (pltpu.VMEM((16, BLOCK_ROWS, 128), bf16), pltpu.VMEM((STATE_ROWS, 128), bf16)),
         8,
         [pltpu.VMEM((BLOCK_ROWS, 128), bf16)],
     )(at, *map(far, (vf, of, vw, ow, v1, v2, o1, o2)))
     got = exchange(blocks, FS)
     got, weights = lax.optimization_barrier((got, weights))
-    other = partner(got[:, :FACTOR_ROWS])
-    along_y = jnp.stack(shifted(weights, "fs_1"))
-    parts = shifted(along_y, "fs_0")
-
-    kept, sent = call(
+    other = partner(got)
+    along_y = jnp.stack([weights] + [shift(weights, "fs_1", d) for d in (1, 2, 3)])
+    before = shift(along_y, "fs_0", 1)
+    after = shift(along_y, "fs_0", 3)
+
+    kept, sent, fv, fo = call(
         tokens_body,
-        (pltpu.VMEM((16, 4, 16, 384), f32), pltpu.VMEM((16, 4, 16, 384), bf16)),
+        (
+            pltpu.VMEM((16, 4, 16, 384), f32),
+            pltpu.VMEM((16, 4, 16, 384), bf16),
+            pltpu.VMEM((D, R), bf16),
+            pltpu.VMEM((DM, R), bf16),
+        ),
         2,
         [
-            pltpu.VMEM((D, R), bf16),
-            pltpu.VMEM((DM, R), bf16),
             pltpu.VMEM((R, D + DM), f32),
             pltpu.VMEM((x.shape[0], R), bf16),
             pltpu.VMEM((x.shape[0], R), bf16),
@@ -346,6 +356,7 @@
     came = partner(sent)
     tiles = (kept + came.astype(f32)).astype(bf16)
     tiles = exchange(tiles.reshape(64, 16, 384), CHIPS)
+    pair = pltpu.VMEM((2, STATE_ROWS, 128), bf16)
     replies = call(
         reply_body,
         pltpu.VMEM((64, 16, 128), f32),
@@ -353,10 +364,13 @@
         [pltpu.VMEM((16, 384), f32), pltpu.VMEM((4, 16, 128), f32)],
         smem=0,
     )(near(tiles))
+    up, down = call(halves_body, (pair, pair), 3, smem=0)(near(replies), near(before), near(after))
+    up = shift(up, "fs_0", 1)
+    down = shift(down, "fs_0", 3)
     back = exchange(replies, CHIPS).reshape(16, 4, 16, 128)
     back = near(back)
-    weights = call(place_body, pltpu.VMEM((16, WEIGHT_ROWS, 128), bf16), 4)(
-        at, *[near(p) for p in parts]
+    weights = call(place_body, pltpu.VMEM((16, STATE_ROWS, 128), bf16), 5)(
+        at, *map(near, (along_y, before, up, down, after))
     )
     came = partner(call(hand_body, pltpu.VMEM((16, 2, 16, 128), f32), 1, smem=0)(back))
 
@@ -380,13 +394,11 @@
         11,
         [
             pltpu.VMEM((R, 384), f32),
-            pltpu.VMEM((D, R), bf16),
-            pltpu.VMEM((DM, R), bf16),
             pltpu.VMEM((R, 768), bf16),
             pltpu.VMEM((D, 128), f32),
             pltpu.VMEM((DM, 256), f32),
         ],
-    )(at, back, near(came), near(got), near(other), near(weights), vw, ow, v1, v2, o1, o2)
+    )(at, back, near(came), near(fv), near(fo), near(weights), vw, ow, v1, v2, o1, o2)
 
 
 def solution(mesh):

time: 106 us -> 103 us (0.972)
  blocking collectives: 49.4 us -> 45 us
  starting transfers between devices: 15.5 us -> 17.3 us
    all_to_all x2, blocking collectives: 49.4 us -> 45 us  [exchange(): return lax.all_to_all(tiles, axis, split_axis=0, concat_axis=0, tiled=True)]
    ppermute x6 -> x7, starting transfers between devices: 10.5 us -> 12.4 us  [shift(): return lax.ppermute(x, axis, [(i, (i + d) % 4) for i in range(4)])]
    ppermute x6 -> x7, waiting for transfers between devices: 17 us -> 16.7 us  [shift(): return lax.ppermute(x, axis, [(i, (i + d) % 4) for i in range(4)])]
    pallas_call x6 -> x7, Pallas kernels: 17.9 us -> 17.8 us  [run(): return call_of(body, *args, **kwargs)(*operands)]
  transfers between devices with their start and end apart: 10 -> 11, of which waited for: 7 -> 7; matrix products, arithmetic and copies ran while one was open for 0% -> 0% of each run, Pallas kernels for 1% -> 2%
where the time goes in v3:
time: 103 us; the launch traced here: 102 us
  blocking collectives  45 us (44%)
  waiting for transfers between devices  21.1 us (20%)
  Pallas kernels  17.8 us (17%)
  starting transfers between devices  17.3 us (17%)
    all_to_all x2, blocking collectives, exchange(): return lax.all_to_all(tiles, axis, split_axis=0, concat_axis=0, tiled=True)  45 us
    pallas_call x7, Pallas kernels, run(): return call_of(body, *args, **kwargs)(*operands)  17.8 us
    ppermute x7, waiting for transfers between devices, shift(): return lax.ppermute(x, axis, [(i, (i + d) % 4) for i in range(4)])  16.7 us
    ppermute x7, starting transfers between devices, shift(): return lax.ppermute(x, axis, [(i, (i + d) % 4) for i in range(4)])  12.4 us
    all_to_all x1, starting transfers between devices, exchange(): return lax.all_to_all(tiles, axis, split_axis=0, concat_axis=0, tiled=True)  4.64 us
    ppermute x3, waiting for transfers between devices, partner(): return lax.ppermute(x, CORE, [(0, 1), (1, 0)])  4.44 us
  transfers between devices with their start and end apart: 11, of which 7 were waited for; matrix products, arithmetic and copies ran while one was open for 0% of the time, Pallas kernels for 2%

profile of v3, /device:TPU:0, one launch (start us, length us, event | category | flops | bytes accessed | tf_op | source)
XLA Modules:
  0.0 102.5 jit_solution(5660882965240115135)
XLA Ops:
  0.7 0.1 pad_add_fusion.at
  0.7 1.1 %shard_map.195 = (bf16[16,192,128]{2,1,0:T(8,128)(2,1)S(1)}, bf16[352,128]{1,0:T(8,128)(2,1)S(1)}) custom-call(s32[3]{0:T(128)S(1)} %pad_add_fusion.at, bf16[128,256]{1,0:T(8,128)(2,1)} %vf.1, bf16[64,256]{1,0:T(8,128)(2,1)} %of.1, f32[128,128]{1,0:T(8,128)} %vw.3, f32[64,256]{1,0:T(8,128)} %ow.3, f32[16,128]{1,0:T(8,128)} %v1.3, f32[16,128]{1,0:T(8,128)} %v2.3, ...), custom_call_target="tpu_custom_call" | custom-call | tf_op jit(solution)/shard_map/pallas_call | solution.py:59
  1.8 22.3 %all_to_all.15.mine = bf16[16,192,128]{2,1,0:T(8,128)(2,1)S(1)} all-to-all(bf16[16,192,128]{2,1,0:T(8,128)(2,1)S(1)} %get-tuple-element.20), channel_id=1, replica_groups=mesh['fs_0'=4,'fs_1'=4,'tp_0'=4,'tp_1'=2] {'fs_0','fs_1'}, dimensions={0} | all-to-all | bytes 1572864 | tf_op jit(solution)/shard_map/all_to_all | solution.py:38
  24.1 2.3 %collective-permute-done.other = bf16[16,192,128]{2,1,0:T(8,128)(2,1)S(1)} collective-permute-done((bf16[16,192,128]{2,1,0:T(8,128)(2,1)S(1)}, bf16[16,192,128]{2,1,0:T(8,128)(2,1)S(1)}, u32[]{:S(2)}, u32[]{:S(2)}) %collective-permute-start) | collective-permute-done | bytes 786464 | tf_op jit(solution)/shard_map/ppermute | solution.py:54
  26.4 11.0 %shard_map.196 = (f32[16,4,16,384]{3,2,1,0:T(8,128)S(1)}, bf16[16,4,16,384]{3,2,1,0:T(8,128)(2,1)S(1)}, bf16[2048,256]{1,0:T(8,128)(2,1)S(1)}, bf16[1024,256]{1,0:T(8,128)(2,1)S(1)}) custom-call(s32[3]{0:T(128)S(1)} %pad_add_fusion.at, bf16[16,192,128]{2,1,0:T(8,128)(2,1)S(1)} %all_to_all.15.mine, bf16[16,192,128]{2,1,0:T(8,128)(2,1)S(1)} %collective-permute-done.other, ...), custom_call_target="tpu_custom_call" | custom-call | flops 12884901888 | tf_op jit(solution)/shard_map/pallas_call | solution.py:59
  37.4 0.2 collective-permute-start.1
  37.6 2.2 %collective-permute-done.1 = bf16[16,4,16,384]{3,2,1,0:T(8,128)(2,1)S(1)} collective-permute-done((bf16[16,4,16,384]{3,2,1,0:T(8,128)(2,1)S(1)}, bf16[16,4,16,384]{3,2,1,0:T(8,128)(2,1)S(1)}, u32[]{:S(2)}, u32[]{:S(2)}) %collective-permute-start.1) | collective-permute-done | bytes 786464 | tf_op jit(solution)/shard_map/ppermute | solution.py:54
  39.8 0.2 add_convert_fusion
  40.0 22.7 %all_to_all.16.tiles = bf16[64,16,384]{2,1,0:T(8,128)(2,1)S(1)} all-to-all(bf16[64,16,384]{2,1,0:T(8,128)(2,1)S(1)} %bitcast.12), channel_id=1, replica_groups=mesh['fs_0'=4,'fs_1'=4,'tp_0'=4,'tp_1'=2] {'fs_0','fs_1','tp_0'}, dimensions={0} | all-to-all | bytes 1572864 | tf_op jit(solution)/shard_map/all_to_all | solution.py:38
  62.7 1.1 %shard_map.197.replies = f32[64,16,128]{2,1,0:T(8,128)} custom-call(bf16[64,16,384]{2,1,0:T(8,128)(2,1)S(1)} %all_to_all.16.tiles), custom_call_target="tpu_custom_call" | custom-call | tf_op jit(solution)/shard_map/pallas_call | solution.py:59
  63.8 4.6 %all-to-all-start.2 = ((f32[64,16,128]{2,1,0:T(8,128)}), f32[64,16,128]{2,1,0:T(8,128)S(1)}, u32[]{:S(2)}, u32[]{:S(2)}) async-start(f32[64,16,128]{2,1,0:T(8,128)} %shard_map.197.replies), calls=%async_computation.2 | async-start | bytes 1048576 | tf_op jit(solution)/shard_map/all_to_all | solution.py:38
  68.5 1.6 %collective-permute-start.3 = (bf16[352,128]{1,0:T(8,128)(2,1)S(1)}, bf16[352,128]{1,0:T(8,128)(2,1)S(1)}, u32[]{:S(2)}, u32[]{:S(2)}) collective-permute-start(bf16[352,128]{1,0:T(8,128)(2,1)S(1)} %get-tuple-element.27), channel_id=1, source_target_pairs={{0,8},{8,16},{16,24},{24,0},{1,9},{9,17},{17,25},{25,1},{2,10},{10... | collective-permute-start | bytes 270344 | tf_op jit(solution)/shard_map/ppermute | solution.py:42
  70.1 2.7 %collective-permute-start.4 = (bf16[352,128]{1,0:T(8,128)(2,1)S(1)}, bf16[352,128]{1,0:T(8,128)(2,1)S(1)}, u32[]{:S(2)}, u32[]{:S(2)}) collective-permute-start(bf16[352,128]{1,0:T(8,128)(2,1)S(1)} %get-tuple-element.27), channel_id=1, source_target_pairs={{0,16},{8,24},{16,0},{24,8},{1,17},{9,25},{17,1},{25,9},{2,18},{10... | collective-permute-start | bytes 270344 | tf_op jit(solution)/shard_map/ppermute | solution.py:42
  72.8 1.5 %collective-permute-start.5 = (bf16[352,128]{1,0:T(8,128)(2,1)S(1)}, bf16[352,128]{1,0:T(8,128)(2,1)S(1)}, u32[]{:S(2)}, u32[]{:S(2)}) collective-permute-start(bf16[352,128]{1,0:T(8,128)(2,1)S(1)} %get-tuple-element.27), channel_id=1, source_target_pairs={{0,24},{8,0},{16,8},{24,16},{1,25},{9,1},{17,9},{25,17},{2,26},{10... | collective-permute-start | bytes 270344 | tf_op jit(solution)/shard_map/ppermute | solution.py:42
  74.2 4.8 %collective-permute-done.3 = bf16[352,128]{1,0:T(8,128)(2,1)S(1)} collective-permute-done((bf16[352,128]{1,0:T(8,128)(2,1)S(1)}, bf16[352,128]{1,0:T(8,128)(2,1)S(1)}, u32[]{:S(2)}, u32[]{:S(2)}) %collective-permute-start.3) | collective-permute-done | bytes 90144 | tf_op jit(solution)/shard_map/ppermute | solution.py:42
  79.1 1.3 %collective-permute-done.4 = bf16[352,128]{1,0:T(8,128)(2,1)S(1)} collective-permute-done((bf16[352,128]{1,0:T(8,128)(2,1)S(1)}, bf16[352,128]{1,0:T(8,128)(2,1)S(1)}, u32[]{:S(2)}, u32[]{:S(2)}) %collective-permute-start.4) | collective-permute-done | bytes 90144 | tf_op jit(solution)/shard_map/ppermute | solution.py:42
  80.4 1.6 %collective-permute-start.6 = (bf16[4,352,128]{2,1,0:T(8,128)(2,1)S(1)}, bf16[4,352,128]{2,1,0:T(8,128)(2,1)S(1)}, u32[]{:S(2)}, u32[]{:S(2)}) collective-permute-start(bf16[4,352,128]{2,1,0:T(8,128)(2,1)S(1)} %pad_maximum_fusion.w0), channel_id=1, source_target_pairs={{0,32},{32,64},{64,96},{96,0},{1,33},{33,65},{65,97},{97,1},{2,34}... | collective-permute-start | bytes 1081352 | tf_op jit(solution)/shard_map/ppermute | solution.py:42
  82.1 1.7 %collective-permute-start.7 = (bf16[4,352,128]{2,1,0:T(8,128)(2,1)S(1)}, bf16[4,352,128]{2,1,0:T(8,128)(2,1)S(1)}, u32[]{:S(2)}, u32[]{:S(2)}) collective-permute-start(bf16[4,352,128]{2,1,0:T(8,128)(2,1)S(1)} %pad_maximum_fusion.w0), channel_id=1, source_target_pairs={{0,96},{32,0},{64,32},{96,64},{1,97},{33,1},{65,33},{97,65},{2,98}... | collective-permute-start | bytes 1081352 | tf_op jit(solution)/shard_map/ppermute | solution.py:42
  83.7 0.2 shard_map.198
  83.9 0.1 collective-permute-start.2
  84.0 6.8 %collective-permute-done.6.before.w1 = bf16[4,352,128]{2,1,0:T(8,128)(2,1)S(1)} collective-permute-done((bf16[4,352,128]{2,1,0:T(8,128)(2,1)S(1)}, bf16[4,352,128]{2,1,0:T(8,128)(2,1)S(1)}, u32[]{:S(2)}, u32[]{:S(2)}) %collective-permute-start.6) | collective-permute-done | bytes 360480 | tf_op jit(solution)/shard_map/ppermute | solution.py:42
  90.8 1.1 %shard_map.199 = (bf16[2,352,128]{2,1,0:T(8,128)(2,1)S(1)}, bf16[2,352,128]{2,1,0:T(8,128)(2,1)S(1)}) custom-call(f32[64,16,128]{2,1,0:T(8,128)} %shard_map.197.replies, bf16[4,352,128]{2,1,0:T(8,128)(2,1)S(1)} %collective-permute-done.6.before.w1, bf16[4,352,128]{2,1,0:T(8,128)(2,1)S(1)} %collective-permute-done.7.after.w3), custom_call_target="tpu_custom_call" | custom-call | tf_op jit(solution)/shard_map/pallas_call | solution.py:59
  91.9 0.0 copy-start
  91.9 0.0 copy-start.1
  91.9 0.0 copy-start.2
  91.9 0.0 copy-start.3
  91.9 1.6 %collective-permute-start.8 = (bf16[2,352,128]{2,1,0:T(8,128)(2,1)S(1)}, bf16[2,352,128]{2,1,0:T(8,128)(2,1)S(1)}, u32[]{:S(2)}, u32[]{:S(2)}) collective-permute-start(bf16[2,352,128]{2,1,0:T(8,128)(2,1)S(1)} %get-tuple-element.28), channel_id=1, source_target_pairs={{0,32},{32,64},{64,96},{96,0},{1,33},{33,65},{65,97},{97,1},{2,34}... | collective-permute-start | bytes 540680 | tf_op jit(solution)/shard_map/ppermute | solution.py:42
  93.6 1.7 %collective-permute-start.9 = (bf16[2,352,128]{2,1,0:T(8,128)(2,1)S(1)}, bf16[2,352,128]{2,1,0:T(8,128)(2,1)S(1)}, u32[]{:S(2)}, u32[]{:S(2)}) collective-permute-start(bf16[2,352,128]{2,1,0:T(8,128)(2,1)S(1)} %get-tuple-element.29), channel_id=1, source_target_pairs={{0,96},{32,0},{64,32},{96,64},{1,97},{33,1},{65,33},{97,65},{2,98}... | collective-permute-start | bytes 540680 | tf_op jit(solution)/shard_map/ppermute | solution.py:42
  95.2 3.5 %collective-permute-done.8.up = bf16[2,352,128]{2,1,0:T(8,128)(2,1)S(1)} collective-permute-done((bf16[2,352,128]{2,1,0:T(8,128)(2,1)S(1)}, bf16[2,352,128]{2,1,0:T(8,128)(2,1)S(1)}, u32[]{:S(2)}, u32[]{:S(2)}) %collective-permute-start.8) | collective-permute-done | bytes 180256 | tf_op jit(solution)/shard_map/ppermute | solution.py:42
  98.7 0.3 collective-permute-done.9.down
  99.0 0.6 shard_map.200.weights
  99.8 2.7 %shard_map.201 = (f32[128,128]{1,0:T(8,128)}, f32[64,256]{1,0:T(8,128)}, f32[128,128]{1,0:T(8,128)}, f32[64,256]{1,0:T(8,128)}, bf16[2048,128]{1,0:T(8,128)(2,1)...) custom-call(s32[3]{0:T(128)S(1)} %pad_add_fusion.at, ...), custom_call_target="tpu_custom_call" | custom-call | tf_op jit(solution)/shard_map/pallas_call | solution.py:59
  (14 shorter events, 0.1 us)
Async XLA Ops:
  24.1 2.3 %collective-permute-start = (bf16[16,192,128]{2,1,0:T(8,128)(2,1)S(1)}, bf16[16,192,128]{2,1,0:T(8,128)(2,1)S(1)}, u32[]{:S(2)}, u32[]{:S(2)}) collective-permute-start(bf16[16,192,128]{2,1,0:T(8,128)(2,1)S(1)} %all_to_all.15.mine), channel_id=1, source_target_pairs={{0,1},{1,0},{2,3},{3,2},{4,5},{5,4},{6,7},{7,6},{8,9},{9,8},{10,11... | collective-permute-start | bytes 2359304 | tf_op jit(solution)/shard_map/ppermute | solution.py:54
  37.4 2.4 %collective-permute-start.1 = (bf16[16,4,16,384]{3,2,1,0:T(8,128)(2,1)S(1)}, bf16[16,4,16,384]{3,2,1,0:T(8,128)(2,1)S(1)}, u32[]{:S(2)}, u32[]{:S(2)}) collective-permute-start(bf16[16,4,16,384]{3,2,1,0:T(8,128)(2,1)S(1)} %get-tuple-element.24), channel_id=1, source_target_pairs={{0,1},{1,0},{2,3},{3,2},{4,5},{5,4},{6,7},{7,6},{8,9},{9,8},{10,11... | collective-permute-start | bytes 2359304 | tf_op jit(solution)/shard_map/ppermute | solution.py:54
  63.8 19.9 %all-to-all-start.2 = ((f32[64,16,128]{2,1,0:T(8,128)}), f32[64,16,128]{2,1,0:T(8,128)S(1)}, u32[]{:S(2)}, u32[]{:S(2)}) async-start(f32[64,16,128]{2,1,0:T(8,128)} %shard_map.197.replies), calls=%async_computation.2 | async-start | bytes 1048576 | tf_op jit(solution)/shard_map/all_to_all | solution.py:38
  68.5 10.6 %collective-permute-start.3 = (bf16[352,128]{1,0:T(8,128)(2,1)S(1)}, bf16[352,128]{1,0:T(8,128)(2,1)S(1)}, u32[]{:S(2)}, u32[]{:S(2)}) collective-permute-start(bf16[352,128]{1,0:T(8,128)(2,1)S(1)} %get-tuple-element.27), channel_id=1, source_target_pairs={{0,8},{8,16},{16,24},{24,0},{1,9},{9,17},{17,25},{25,1},{2,10},{10... | collective-permute-start | bytes 270344 | tf_op jit(solution)/shard_map/ppermute | solution.py:42
  70.1 10.2 %collective-permute-start.4 = (bf16[352,128]{1,0:T(8,128)(2,1)S(1)}, bf16[352,128]{1,0:T(8,128)(2,1)S(1)}, u32[]{:S(2)}, u32[]{:S(2)}) collective-permute-start(bf16[352,128]{1,0:T(8,128)(2,1)S(1)} %get-tuple-element.27), channel_id=1, source_target_pairs={{0,16},{8,24},{16,0},{24,8},{1,17},{9,25},{17,1},{25,9},{2,18},{10... | collective-permute-start | bytes 270344 | tf_op jit(solution)/shard_map/ppermute | solution.py:42
  72.8 7.6 %collective-permute-start.5 = (bf16[352,128]{1,0:T(8,128)(2,1)S(1)}, bf16[352,128]{1,0:T(8,128)(2,1)S(1)}, u32[]{:S(2)}, u32[]{:S(2)}) collective-permute-start(bf16[352,128]{1,0:T(8,128)(2,1)S(1)} %get-tuple-element.27), channel_id=1, source_target_pairs={{0,24},{8,0},{16,8},{24,16},{1,25},{9,1},{17,9},{25,17},{2,26},{10... | collective-permute-start | bytes 270344 | tf_op jit(solution)/shard_map/ppermute | solution.py:42
  80.4 10.4 %collective-permute-start.6 = (bf16[4,352,128]{2,1,0:T(8,128)(2,1)S(1)}, bf16[4,352,128]{2,1,0:T(8,128)(2,1)S(1)}, u32[]{:S(2)}, u32[]{:S(2)}) collective-permute-start(bf16[4,352,128]{2,1,0:T(8,128)(2,1)S(1)} %pad_maximum_fusion.w0), channel_id=1, source_target_pairs={{0,32},{32,64},{64,96},{96,0},{1,33},{33,65},{65,97},{97,1},{2,34}... | collective-permute-start | bytes 1081352 | tf_op jit(solution)/shard_map/ppermute | solution.py:42
  82.1 8.7 %collective-permute-start.7 = (bf16[4,352,128]{2,1,0:T(8,128)(2,1)S(1)}, bf16[4,352,128]{2,1,0:T(8,128)(2,1)S(1)}, u32[]{:S(2)}, u32[]{:S(2)}) collective-permute-start(bf16[4,352,128]{2,1,0:T(8,128)(2,1)S(1)} %pad_maximum_fusion.w0), channel_id=1, source_target_pairs={{0,96},{32,0},{64,32},{96,64},{1,97},{33,1},{65,33},{97,65},{2,98}... | collective-permute-start | bytes 1081352 | tf_op jit(solution)/shard_map/ppermute | solution.py:42
  83.9 15.8 %collective-permute-start.2 = (f32[16,2,16,128]{3,2,1,0:T(8,128)S(1)}, f32[16,2,16,128]{3,2,1,0:T(8,128)S(1)}, u32[]{:S(2)}, u32[]{:S(2)}) collective-permute-start(f32[16,2,16,128]{3,2,1,0:T(8,128)S(1)} %shard_map.198), channel_id=1, source_target_pairs={{0,1},{1,0},{2,3},{3,2},{4,5},{5,4},{6,7},{7,6},{8,9},{9,8},{10,11... | collective-permute-start | bytes 786440 | tf_op jit(solution)/shard_map/ppermute | solution.py:54
  91.9 7.8 %copy-start = (f32[128,128]{1,0:T(8,128)S(1)}, f32[128,128]{1,0:T(8,128)}, u32[]{:S(2)}) copy-start(f32[128,128]{1,0:T(8,128)} %vw.3) | copy-start | bytes 196612
  91.9 7.8 %copy-start.1 = (f32[64,256]{1,0:T(8,128)S(1)}, f32[64,256]{1,0:T(8,128)}, u32[]{:S(2)}) copy-start(f32[64,256]{1,0:T(8,128)} %ow.3) | copy-start | bytes 196612
  91.9 7.8 %copy-start.2 = (f32[16,256]{1,0:T(8,128)S(1)}, f32[16,256]{1,0:T(8,128)}, u32[]{:S(2)}) copy-start(f32[16,256]{1,0:T(8,128)} %o1.3) | copy-start | bytes 49156
  91.9 7.8 %copy-start.3 = (f32[16,256]{1,0:T(8,128)S(1)}, f32[16,256]{1,0:T(8,128)}, u32[]{:S(2)}) copy-start(f32[16,256]{1,0:T(8,128)} %o2.3) | copy-start | bytes 49156
  91.9 7.8 %copy-start.4 = (f32[16,128]{1,0:T(8,128)S(1)}, f32[16,128]{1,0:T(8,128)}, u32[]{:S(2)}) copy-start(f32[16,128]{1,0:T(8,128)} %v1.3) | copy-start | bytes 24580
  91.9 7.8 %copy-start.5 = (f32[16,128]{1,0:T(8,128)S(1)}, f32[16,128]{1,0:T(8,128)}, u32[]{:S(2)}) copy-start(f32[16,128]{1,0:T(8,128)} %v2.3) | copy-start | bytes 24580
  91.9 6.8 %collective-permute-start.8 = (bf16[2,352,128]{2,1,0:T(8,128)(2,1)S(1)}, bf16[2,352,128]{2,1,0:T(8,128)(2,1)S(1)}, u32[]{:S(2)}, u32[]{:S(2)}) collective-permute-start(bf16[2,352,128]{2,1,0:T(8,128)(2,1)S(1)} %get-tuple-element.28), channel_id=1, source_target_pairs={{0,32},{32,64},{64,96},{96,0},{1,33},{33,65},{65,97},{97,1},{2,34}... | collective-permute-start | bytes 540680 | tf_op jit(solution)/shard_map/ppermute | solution.py:42
  93.6 5.5 %collective-permute-start.9 = (bf16[2,352,128]{2,1,0:T(8,128)(2,1)S(1)}, bf16[2,352,128]{2,1,0:T(8,128)(2,1)S(1)}, u32[]{:S(2)}, u32[]{:S(2)}) collective-permute-start(bf16[2,352,128]{2,1,0:T(8,128)(2,1)S(1)} %get-tuple-element.29), channel_id=1, source_target_pairs={{0,96},{32,0},{64,32},{96,64},{1,97},{33,1},{65,33},{97,65},{2,98}... | collective-permute-start | bytes 540680 | tf_op jit(solution)/shard_map/ppermute | solution.py:42

commit v4 on v3

--- a/solution.py
+++ b/solution.py
@@ -96,17 +96,13 @@
     state[336:352] = o2[:, 128:].astype(bf16)
 
 
-def place_body(at, w0, w1, up, down, w3, out):
+def place_body(at, w0, w1, w2, w3, out):
     row = at[1]
     for dz in range(4):
         for dy in range(4):
             from_z = jnp.bitwise_and(row // 4 - dz, 3)
             from_y = jnp.bitwise_and(row - dy, 3)
-            if dz == 2:
-                part = up[dy] if dy < 2 else down[dy - 2]
-            else:
-                part = (w0, w1, None, w3)[dz][dy]
-            out[4 * from_z + from_y] = part
+            out[4 * from_z + from_y] = (w0, w1, w2, w3)[dz][dy]
 
 
 def join_factors(mine, other, fv, fo):
@@ -217,9 +213,8 @@
     arrange(acc, 0, at[0], kept)
 
 
-def halves_body(replies, before, after, up, down):
-    up[...] = before[0:2]
-    down[...] = after[2:4]
+def onward_body(replies, before, up):
+    up[...] = before[...]
 
 
 def reply_body(tiles, out, own, stage):
@@ -356,7 +351,6 @@
     came = partner(sent)
     tiles = (kept + came.astype(f32)).astype(bf16)
     tiles = exchange(tiles.reshape(64, 16, 384), CHIPS)
-    pair = pltpu.VMEM((2, STATE_ROWS, 128), bf16)
     replies = call(
         reply_body,
         pltpu.VMEM((64, 16, 128), f32),
@@ -364,13 +358,13 @@
         [pltpu.VMEM((16, 384), f32), pltpu.VMEM((4, 16, 128), f32)],
         smem=0,
     )(near(tiles))
-    up, down = call(halves_body, (pair, pair), 3, smem=0)(near(replies), near(before), near(after))
-    up = shift(up, "fs_0", 1)
-    down = shift(down, "fs_0", 3)
+    line = pltpu.VMEM((4, STATE_ROWS, 128), bf16)
+    onward = call(onward_body, line, 2, smem=0)(near(replies), near(before))
+    onward = shift(onward, "fs_0", 1)
     back = exchange(replies, CHIPS).reshape(16, 4, 16, 128)
     back = near(back)
-    weights = call(place_body, pltpu.VMEM((16, STATE_ROWS, 128), bf16), 5)(
-        at, *map(near, (along_y, before, up, down, after))
+    weights = call(place_body, pltpu.VMEM((16, STATE_ROWS, 128), bf16), 4)(
+        at, *map(near, (along_y, before, onward, after))
     )
     came = partner(call(hand_body, pltpu.VMEM((16, 2, 16, 128), f32), 1, smem=0)(back))
 

time: 103 us -> 102 us (level)
  blocking collectives: 45 us -> 22.3 us
  waiting for transfers between devices: 21.1 us -> 37.2 us
  starting transfers between devices: 17.3 us -> 20.6 us
    all_to_all x2 -> x1, blocking collectives: 45 us -> 22.3 us  [exchange(): return lax.all_to_all(tiles, axis, split_axis=0, concat_axis=0, tiled=True)]
    all_to_all x1 -> x2, waiting for transfers between devices: 0.01 us -> 10.8 us  [exchange(): return lax.all_to_all(tiles, axis, split_axis=0, concat_axis=0, tiled=True)]
    all_to_all x1 -> x2, starting transfers between devices: 4.64 us -> 11.2 us  [exchange(): return lax.all_to_all(tiles, axis, split_axis=0, concat_axis=0, tiled=True)]
    ppermute x7 -> x6, waiting for transfers between devices: 16.7 us -> 22 us  [shift(): return lax.ppermute(x, axis, [(i, (i + d) % 4) for i in range(4)])]
    ppermute x7 -> x6, starting transfers between devices: 12.4 us -> 9.09 us  [shift(): return lax.ppermute(x, axis, [(i, (i + d) % 4) for i in range(4)])]
  transfers between devices with their start and end apart: 11 -> 11, of which waited for: 7 -> 5; matrix products, arithmetic and copies ran while one was open for 0% -> 0% of each run, Pallas kernels for 2% -> 4%
where the time goes in v4:
time: 102 us; the launch traced here: 101 us
  waiting for transfers between devices  37.2 us (36%)
  blocking collectives  22.3 us (22%)
  starting transfers between devices  20.6 us (20%)
  Pallas kernels  18.6 us (18%)
  other arithmetic  1.28 us (1%)
    all_to_all x1, blocking collectives, exchange(): return lax.all_to_all(tiles, axis, split_axis=0, concat_axis=0, tiled=True)  22.3 us
    ppermute x6, waiting for transfers between devices, shift(): return lax.ppermute(x, axis, [(i, (i + d) % 4) for i in range(4)])  22 us
    pallas_call x7, Pallas kernels, run(): return call_of(body, *args, **kwargs)(*operands)  18.6 us
    all_to_all x2, starting transfers between devices, exchange(): return lax.all_to_all(tiles, axis, split_axis=0, concat_axis=0, tiled=True)  11.2 us
    all_to_all x2, waiting for transfers between devices, exchange(): return lax.all_to_all(tiles, axis, split_axis=0, concat_axis=0, tiled=True)  10.8 us
    ppermute x6, starting transfers between devices, shift(): return lax.ppermute(x, axis, [(i, (i + d) % 4) for i in range(4)])  9.09 us
    ppermute x3, waiting for transfers between devices, partner(): return lax.ppermute(x, CORE, [(0, 1), (1, 0)])  4.44 us
  transfers between devices with their start and end apart: 11, of which 5 were waited for; matrix products, arithmetic and copies ran while one was open for 0% of the time, Pallas kernels for 4%

profile of v4, /device:TPU:0, one launch (start us, length us, event | category | flops | bytes accessed | tf_op | source)
XLA Modules:
  0.0 100.8 jit_solution(8452727120445116135)
XLA Ops:
  0.7 0.1 pad_add_fusion.at
  0.7 1.1 %shard_map.195 = (bf16[16,192,128]{2,1,0:T(8,128)(2,1)S(1)}, bf16[352,128]{1,0:T(8,128)(2,1)S(1)}) custom-call(s32[3]{0:T(128)S(1)} %pad_add_fusion.at, bf16[128,256]{1,0:T(8,128)(2,1)} %vf.1, bf16[64,256]{1,0:T(8,128)(2,1)} %of.1, f32[128,128]{1,0:T(8,128)} %vw.3, f32[64,256]{1,0:T(8,128)} %ow.3, f32[16,128]{1,0:T(8,128)} %v1.3, f32[16,128]{1,0:T(8,128)} %v2.3, ...), custom_call_target="tpu_custom_call" | custom-call | tf_op jit(solution)/shard_map/pallas_call | solution.py:59
  1.8 22.3 %all_to_all.15.mine = bf16[16,192,128]{2,1,0:T(8,128)(2,1)S(1)} all-to-all(bf16[16,192,128]{2,1,0:T(8,128)(2,1)S(1)} %get-tuple-element.18), channel_id=1, replica_groups=mesh['fs_0'=4,'fs_1'=4,'tp_0'=4,'tp_1'=2] {'fs_0','fs_1'}, dimensions={0} | all-to-all | bytes 1572864 | tf_op jit(solution)/shard_map/all_to_all | solution.py:38
  24.1 2.3 %collective-permute-done.other = bf16[16,192,128]{2,1,0:T(8,128)(2,1)S(1)} collective-permute-done((bf16[16,192,128]{2,1,0:T(8,128)(2,1)S(1)}, bf16[16,192,128]{2,1,0:T(8,128)(2,1)S(1)}, u32[]{:S(2)}, u32[]{:S(2)}) %collective-permute-start) | collective-permute-done | bytes 786464 | tf_op jit(solution)/shard_map/ppermute | solution.py:54
  26.4 11.0 %shard_map.196 = (f32[16,4,16,384]{3,2,1,0:T(8,128)S(1)}, bf16[16,4,16,384]{3,2,1,0:T(8,128)(2,1)S(1)}, bf16[2048,256]{1,0:T(8,128)(2,1)S(1)}, bf16[1024,256]{1,0:T(8,128)(2,1)S(1)}) custom-call(s32[3]{0:T(128)S(1)} %pad_add_fusion.at, bf16[16,192,128]{2,1,0:T(8,128)(2,1)S(1)} %all_to_all.15.mine, bf16[16,192,128]{2,1,0:T(8,128)(2,1)S(1)} %collective-permute-done.other, ...), custom_call_target="tpu_custom_call" | custom-call | flops 12884901888 | tf_op jit(solution)/shard_map/pallas_call | solution.py:59
  37.4 0.2 collective-permute-start.1
  37.6 2.2 %collective-permute-done.1 = bf16[16,4,16,384]{3,2,1,0:T(8,128)(2,1)S(1)} collective-permute-done((bf16[16,4,16,384]{3,2,1,0:T(8,128)(2,1)S(1)}, bf16[16,4,16,384]{3,2,1,0:T(8,128)(2,1)S(1)}, u32[]{:S(2)}, u32[]{:S(2)}) %collective-permute-start.1) | collective-permute-done | bytes 786464 | tf_op jit(solution)/shard_map/ppermute | solution.py:54
  39.8 1.2 %add_convert_fusion = bf16[16,4,16,384]{3,2,1,0:T(8,128)(2,1)} fusion(f32[16,4,16,384]{3,2,1,0:T(8,128)S(1)} %get-tuple-element.21, bf16[16,4,16,384]{3,2,1,0:T(8,128)(2,1)S(1)} %collective-permute-done.1), kind=kLoop, calls=%fused_computation | loop fusion | flops 1179648 | bytes 3145728 | tf_op jit(solution)/shard_map/convert_element_type | solution.py:352
  41.0 6.5 %all-to-all-start.1 = ((bf16[64,16,384]{2,1,0:T(8,128)(2,1)}), bf16[64,16,384]{2,1,0:T(8,128)(2,1)S(1)}, u32[]{:S(2)}, u32[]{:S(2)}) async-start(bf16[64,16,384]{2,1,0:T(8,128)(2,1)} %bitcast.12), calls=%async_computation.1 | async-start | bytes 1572864 | tf_op jit(solution)/shard_map/all_to_all | solution.py:38
  47.4 1.6 %collective-permute-start.3 = (bf16[352,128]{1,0:T(8,128)(2,1)S(1)}, bf16[352,128]{1,0:T(8,128)(2,1)S(1)}, u32[]{:S(2)}, u32[]{:S(2)}) collective-permute-start(bf16[352,128]{1,0:T(8,128)(2,1)S(1)} %get-tuple-element.25), channel_id=1, source_target_pairs={{0,8},{8,16},{16,24},{24,0},{1,9},{9,17},{17,25},{25,1},{2,10},{10... | collective-permute-start | bytes 270344 | tf_op jit(solution)/shard_map/ppermute | solution.py:42
  49.1 2.7 %collective-permute-start.4 = (bf16[352,128]{1,0:T(8,128)(2,1)S(1)}, bf16[352,128]{1,0:T(8,128)(2,1)S(1)}, u32[]{:S(2)}, u32[]{:S(2)}) collective-permute-start(bf16[352,128]{1,0:T(8,128)(2,1)S(1)} %get-tuple-element.25), channel_id=1, source_target_pairs={{0,16},{8,24},{16,0},{24,8},{1,17},{9,25},{17,1},{25,9},{2,18},{10... | collective-permute-start | bytes 270344 | tf_op jit(solution)/shard_map/ppermute | solution.py:42
  51.8 1.5 %collective-permute-start.5 = (bf16[352,128]{1,0:T(8,128)(2,1)S(1)}, bf16[352,128]{1,0:T(8,128)(2,1)S(1)}, u32[]{:S(2)}, u32[]{:S(2)}) collective-permute-start(bf16[352,128]{1,0:T(8,128)(2,1)S(1)} %get-tuple-element.25), channel_id=1, source_target_pairs={{0,24},{8,0},{16,8},{24,16},{1,25},{9,1},{17,9},{25,17},{2,26},{10... | collective-permute-start | bytes 270344 | tf_op jit(solution)/shard_map/ppermute | solution.py:42
  53.2 10.8 %all-to-all-done.1.tiles = bf16[64,16,384]{2,1,0:T(8,128)(2,1)S(1)} async-done(((bf16[64,16,384]{2,1,0:T(8,128)(2,1)}), bf16[64,16,384]{2,1,0:T(8,128)(2,1)S(1)}, u32[]{:S(2)}, u32[]{:S(2)}) %all-to-all-start.1) | async-done | bytes 786464 | tf_op jit(solution)/shard_map/all_to_all | solution.py:38
  64.0 1.1 %shard_map.197.replies = f32[64,16,128]{2,1,0:T(8,128)} custom-call(bf16[64,16,384]{2,1,0:T(8,128)(2,1)S(1)} %all-to-all-done.1.tiles), custom_call_target="tpu_custom_call" | custom-call | tf_op jit(solution)/shard_map/pallas_call | solution.py:59
  65.1 4.8 %all-to-all-start.2 = ((f32[64,16,128]{2,1,0:T(8,128)}), f32[64,16,128]{2,1,0:T(8,128)S(1)}, u32[]{:S(2)}, u32[]{:S(2)}) async-start(f32[64,16,128]{2,1,0:T(8,128)} %shard_map.197.replies), calls=%async_computation.2 | async-start | bytes 1048576 | tf_op jit(solution)/shard_map/all_to_all | solution.py:38
  69.8 0.0 collective-permute-done.3
  69.8 0.0 collective-permute-done.4
  69.9 1.6 %collective-permute-start.6 = (bf16[4,352,128]{2,1,0:T(8,128)(2,1)S(1)}, bf16[4,352,128]{2,1,0:T(8,128)(2,1)S(1)}, u32[]{:S(2)}, u32[]{:S(2)}) collective-permute-start(bf16[4,352,128]{2,1,0:T(8,128)(2,1)S(1)} %pad_maximum_fusion.w0), channel_id=1, source_target_pairs={{0,32},{32,64},{64,96},{96,0},{1,33},{33,65},{65,97},{97,1},{2,34}... | collective-permute-start | bytes 1081352 | tf_op jit(solution)/shard_map/ppermute | solution.py:42
  71.6 1.7 %collective-permute-start.8 = (bf16[4,352,128]{2,1,0:T(8,128)(2,1)S(1)}, bf16[4,352,128]{2,1,0:T(8,128)(2,1)S(1)}, u32[]{:S(2)}, u32[]{:S(2)}) collective-permute-start(bf16[4,352,128]{2,1,0:T(8,128)(2,1)S(1)} %pad_maximum_fusion.w0), channel_id=1, source_target_pairs={{0,96},{32,0},{64,32},{96,64},{1,97},{33,1},{65,33},{97,65},{2,98}... | collective-permute-start | bytes 1081352 | tf_op jit(solution)/shard_map/ppermute | solution.py:42
  73.2 12.2 %collective-permute-done.6.before.w1 = bf16[4,352,128]{2,1,0:T(8,128)(2,1)S(1)} collective-permute-done((bf16[4,352,128]{2,1,0:T(8,128)(2,1)S(1)}, bf16[4,352,128]{2,1,0:T(8,128)(2,1)S(1)}, u32[]{:S(2)}, u32[]{:S(2)}) %collective-permute-start.6) | collective-permute-done | bytes 360480 | tf_op jit(solution)/shard_map/ppermute | solution.py:42
  85.4 1.8 %shard_map.199 = bf16[4,352,128]{2,1,0:T(8,128)(2,1)} custom-call(f32[64,16,128]{2,1,0:T(8,128)} %shard_map.197.replies, bf16[4,352,128]{2,1,0:T(8,128)(2,1)S(1)} %collective-permute-done.6.before.w1), custom_call_target="tpu_custom_call" | custom-call | tf_op jit(solution)/shard_map/pallas_call | solution.py:59
  87.2 0.2 shard_map.198
  87.5 0.0 copy-start
  87.5 0.0 copy-start.1
  87.5 0.0 copy-start.2
  87.5 0.0 copy-start.3
  87.5 0.0 copy-start.4
  87.5 0.0 copy-start.5
  87.5 0.1 collective-permute-start.2
  87.6 9.7 %collective-permute-done.7.w2 = bf16[4,352,128]{2,1,0:T(8,128)(2,1)S(1)} collective-permute-done((bf16[4,352,128]{2,1,0:T(8,128)(2,1)}, bf16[4,352,128]{2,1,0:T(8,128)(2,1)S(1)}, u32[]{:S(2)}, u32[]{:S(2)}) %collective-permute-start.7) | collective-permute-done | bytes 360480 | tf_op jit(solution)/shard_map/ppermute | solution.py:42
  97.4 0.6 shard_map.200.weights
  98.1 2.7 %shard_map.201 = (f32[128,128]{1,0:T(8,128)}, f32[64,256]{1,0:T(8,128)}, f32[128,128]{1,0:T(8,128)}, f32[64,256]{1,0:T(8,128)}, bf16[2048,128]{1,0:T(8,128)(2,1)...) custom-call(s32[3]{0:T(128)S(1)} %pad_add_fusion.at, ...), custom_call_target="tpu_custom_call" | custom-call | tf_op jit(solution)/shard_map/pallas_call | solution.py:59
  (13 shorter events, 0.1 us)
Async XLA Ops:
  24.1 2.3 %collective-permute-start = (bf16[16,192,128]{2,1,0:T(8,128)(2,1)S(1)}, bf16[16,192,128]{2,1,0:T(8,128)(2,1)S(1)}, u32[]{:S(2)}, u32[]{:S(2)}) collective-permute-start(bf16[16,192,128]{2,1,0:T(8,128)(2,1)S(1)} %all_to_all.15.mine), channel_id=1, source_target_pairs={{0,1},{1,0},{2,3},{3,2},{4,5},{5,4},{6,7},{7,6},{8,9},{9,8},{10,11... | collective-permute-start | bytes 2359304 | tf_op jit(solution)/shard_map/ppermute | solution.py:54
  37.4 2.4 %collective-permute-start.1 = (bf16[16,4,16,384]{3,2,1,0:T(8,128)(2,1)S(1)}, bf16[16,4,16,384]{3,2,1,0:T(8,128)(2,1)S(1)}, u32[]{:S(2)}, u32[]{:S(2)}) collective-permute-start(bf16[16,4,16,384]{3,2,1,0:T(8,128)(2,1)S(1)} %get-tuple-element.22), channel_id=1, source_target_pairs={{0,1},{1,0},{2,3},{3,2},{4,5},{5,4},{6,7},{7,6},{8,9},{9,8},{10,11... | collective-permute-start | bytes 2359304 | tf_op jit(solution)/shard_map/ppermute | solution.py:54
  41.0 23.0 %all-to-all-start.1 = ((bf16[64,16,384]{2,1,0:T(8,128)(2,1)}), bf16[64,16,384]{2,1,0:T(8,128)(2,1)S(1)}, u32[]{:S(2)}, u32[]{:S(2)}) async-start(bf16[64,16,384]{2,1,0:T(8,128)(2,1)} %bitcast.12), calls=%async_computation.1 | async-start | bytes 1572864 | tf_op jit(solution)/shard_map/all_to_all | solution.py:38
  47.4 22.4 %collective-permute-start.3 = (bf16[352,128]{1,0:T(8,128)(2,1)S(1)}, bf16[352,128]{1,0:T(8,128)(2,1)S(1)}, u32[]{:S(2)}, u32[]{:S(2)}) collective-permute-start(bf16[352,128]{1,0:T(8,128)(2,1)S(1)} %get-tuple-element.25), channel_id=1, source_target_pairs={{0,8},{8,16},{16,24},{24,0},{1,9},{9,17},{17,25},{25,1},{2,10},{10... | collective-permute-start | bytes 270344 | tf_op jit(solution)/shard_map/ppermute | solution.py:42
  49.1 20.8 %collective-permute-start.4 = (bf16[352,128]{1,0:T(8,128)(2,1)S(1)}, bf16[352,128]{1,0:T(8,128)(2,1)S(1)}, u32[]{:S(2)}, u32[]{:S(2)}) collective-permute-start(bf16[352,128]{1,0:T(8,128)(2,1)S(1)} %get-tuple-element.25), channel_id=1, source_target_pairs={{0,16},{8,24},{16,0},{24,8},{1,17},{9,25},{17,1},{25,9},{2,18},{10... | collective-permute-start | bytes 270344 | tf_op jit(solution)/shard_map/ppermute | solution.py:42
  51.8 18.1 %collective-permute-start.5 = (bf16[352,128]{1,0:T(8,128)(2,1)S(1)}, bf16[352,128]{1,0:T(8,128)(2,1)S(1)}, u32[]{:S(2)}, u32[]{:S(2)}) collective-permute-start(bf16[352,128]{1,0:T(8,128)(2,1)S(1)} %get-tuple-element.25), channel_id=1, source_target_pairs={{0,24},{8,0},{16,8},{24,16},{1,25},{9,1},{17,9},{25,17},{2,26},{10... | collective-permute-start | bytes 270344 | tf_op jit(solution)/shard_map/ppermute | solution.py:42
  65.1 22.2 %all-to-all-start.2 = ((f32[64,16,128]{2,1,0:T(8,128)}), f32[64,16,128]{2,1,0:T(8,128)S(1)}, u32[]{:S(2)}, u32[]{:S(2)}) async-start(f32[64,16,128]{2,1,0:T(8,128)} %shard_map.197.replies), calls=%async_computation.2 | async-start | bytes 1048576 | tf_op jit(solution)/shard_map/all_to_all | solution.py:38
  69.9 15.5 %collective-permute-start.6 = (bf16[4,352,128]{2,1,0:T(8,128)(2,1)S(1)}, bf16[4,352,128]{2,1,0:T(8,128)(2,1)S(1)}, u32[]{:S(2)}, u32[]{:S(2)}) collective-permute-start(bf16[4,352,128]{2,1,0:T(8,128)(2,1)S(1)} %pad_maximum_fusion.w0), channel_id=1, source_target_pairs={{0,32},{32,64},{64,96},{96,0},{1,33},{33,65},{65,97},{97,1},{2,34}... | collective-permute-start | bytes 1081352 | tf_op jit(solution)/shard_map/ppermute | solution.py:42
  71.6 16.1 %collective-permute-start.8 = (bf16[4,352,128]{2,1,0:T(8,128)(2,1)S(1)}, bf16[4,352,128]{2,1,0:T(8,128)(2,1)S(1)}, u32[]{:S(2)}, u32[]{:S(2)}) collective-permute-start(bf16[4,352,128]{2,1,0:T(8,128)(2,1)S(1)} %pad_maximum_fusion.w0), channel_id=1, source_target_pairs={{0,96},{32,0},{64,32},{96,64},{1,97},{33,1},{65,33},{97,65},{2,98}... | collective-permute-start | bytes 1081352 | tf_op jit(solution)/shard_map/ppermute | solution.py:42
  87.2 10.1 %collective-permute-start.7 = (bf16[4,352,128]{2,1,0:T(8,128)(2,1)}, bf16[4,352,128]{2,1,0:T(8,128)(2,1)S(1)}, u32[]{:S(2)}, u32[]{:S(2)}) collective-permute-start(bf16[4,352,128]{2,1,0:T(8,128)(2,1)} %shard_map.199), channel_id=1, source_target_pairs={{0,32},{32,64},{64,96},{96,0},{1,33},{33,65},{65,97},{97,1},{2,34}... | collective-permute-start | bytes 1081352 | tf_op jit(solution)/shard_map/ppermute | solution.py:42
  87.5 10.6 %copy-start = (f32[128,128]{1,0:T(8,128)S(1)}, f32[128,128]{1,0:T(8,128)}, u32[]{:S(2)}) copy-start(f32[128,128]{1,0:T(8,128)} %vw.3) | copy-start | bytes 196612
  87.5 10.6 %copy-start.1 = (f32[64,256]{1,0:T(8,128)S(1)}, f32[64,256]{1,0:T(8,128)}, u32[]{:S(2)}) copy-start(f32[64,256]{1,0:T(8,128)} %ow.3) | copy-start | bytes 196612
  87.5 10.6 %copy-start.2 = (f32[16,256]{1,0:T(8,128)S(1)}, f32[16,256]{1,0:T(8,128)}, u32[]{:S(2)}) copy-start(f32[16,256]{1,0:T(8,128)} %o1.3) | copy-start | bytes 49156
  87.5 10.6 %copy-start.3 = (f32[16,256]{1,0:T(8,128)S(1)}, f32[16,256]{1,0:T(8,128)}, u32[]{:S(2)}) copy-start(f32[16,256]{1,0:T(8,128)} %o2.3) | copy-start | bytes 49156
  87.5 10.6 %copy-start.4 = (f32[16,128]{1,0:T(8,128)S(1)}, f32[16,128]{1,0:T(8,128)}, u32[]{:S(2)}) copy-start(f32[16,128]{1,0:T(8,128)} %v1.3) | copy-start | bytes 24580
  87.5 10.6 %copy-start.5 = (f32[16,128]{1,0:T(8,128)S(1)}, f32[16,128]{1,0:T(8,128)}, u32[]{:S(2)}) copy-start(f32[16,128]{1,0:T(8,128)} %v2.3) | copy-start | bytes 24580
  87.5 10.5 %collective-permute-start.2 = (f32[16,2,16,128]{3,2,1,0:T(8,128)S(1)}, f32[16,2,16,128]{3,2,1,0:T(8,128)S(1)}, u32[]{:S(2)}, u32[]{:S(2)}) collective-permute-start(f32[16,2,16,128]{3,2,1,0:T(8,128)S(1)} %shard_map.198), channel_id=1, source_target_pairs={{0,1},{1,0},{2,3},{3,2},{4,5},{5,4},{6,7},{7,6},{8,9},{9,8},{10,11... | collective-permute-start | bytes 786440 | tf_op jit(solution)/shard_map/ppermute | solution.py:54
